TPU v7x, 256 devices: a whole 4x4x8 slice. The times are simulated.
256 devices in a mesh: sp: 64 (over z, x, core), tp: 4 (over y).
Axes of the slice: x: 4, y: 4, z: 8, core: 2. Of those that a mesh axis runs over, the one named last changes fastest.
Arguments:
- tokens: bfloat16 [24576, 2048], P(('sp', 'tp')), may hold values from -6 to 6
- norm_gain: float32 [2048], replicated, may hold values from 0.1 to 1.9
- w_recept: bfloat16 [2048, 1024], P(None, 'tp'), may hold values from -0.125 to 0.125
- w_key: bfloat16 [2048, 1024], P(None, 'tp'), may hold values from -0.125 to 0.125
- w_value: bfloat16 [2048, 1024], P(None, 'tp'), may hold values from -0.125 to 0.125
- w_decay: bfloat16 [2048, 1024], P(None, 'tp'), may hold values from -0.125 to 0.125
- w_rate: bfloat16 [2048, 1024], P(None, 'tp'), may hold values from -0.125 to 0.125
- w_gate: bfloat16 [2048, 1024], P(None, 'tp'), may hold values from -0.125 to 0.125
- shift_mix: float32 [3, 1024], P(None, 'tp'), may hold values from 0 to 1
- decay_base: float32 [1024], P('tp'), may hold values from -16 to -2
- rate_base: float32 [1024], P('tp'), may hold values from -10 to 1
- decay_drift: float32 [24576], P('sp'), may hold values from -2 to 2, as said below
- group_gain: float32 [1024], P('tp'), may hold values from 0.1 to 1.9
- initial_state: float32 [16, 64, 64], P('tp'), may hold values from -240 to 240
- w_out: bfloat16 [1024, 2048], replicated, may hold values from -0.1875 to 0.1875
Outputs:
- out: bfloat16 [24576, 2048], P(('sp', 'tp'))
Inputs may be any that keep to these rules, and one draw needn't show every extreme that they name: `decay_drift`: constant over aligned runs of 64 positions.
All inputs are finite; a program needn't handle non-finite values.
Results may differ from a plain program's by a relative error of at most 0.0083.
Values may be sent and summed in bfloat16 or wider, within the bound.
A program may use at most 128 MiB of HBM per device.

v0:
```python
import jax
import jax.numpy as jnp
from jax import lax
from jax.sharding import Mesh
from jax.sharding import PartitionSpec as P

HEAD = 64
BLOCK = 64
SP = ("sp_0", "sp_1", "sp_2")
SP_TP = ("sp_0", "sp_1", "sp_2", "tp")


norm_floor = 0.5
group_floor = 1.0
highest = lax.Precision.HIGHEST


def copy_for_each(shard, axis):
    count = lax.axis_size(axis)
    return lax.all_to_all(
        jnp.broadcast_to(shard[None], (count, *shard.shape)), axis, 0, 0, tiled=True
    )


def in_order(blocks, dim):
    blocks = jnp.moveaxis(blocks, 0, dim)
    lengths = blocks.shape
    return blocks.reshape(*lengths[:dim], lengths[dim] * lengths[dim + 1], *lengths[dim + 2 :])


def gathered_copies(shard, axis, dim):
    blocks = copy_for_each(shard, axis)
    return in_order(blocks, dim)


def shifted_2(block, axis, distance):
    devices = range(lax.axis_size(axis))
    route = [(i - distance, i) for i in devices if i - distance in devices]
    return lax.ppermute(block, axis, route)


def filled_with(shard, identity):
    return jax.tree.map(
        lambda a, e: jnp.broadcast_to(jnp.asarray(e, a.dtype), a.shape), shard, identity
    )


def carried_in(shard, axes, combine, identity):
    before = start = filled_with(shard, identity)
    running = shard
    for axis in reversed(axes):
        count, position = (lax.axis_size(axis), lax.axis_index(axis))
        pieces = jax.tree.map(lambda part: lax.all_gather(part, axis), running)
        inside, running = (start, start)
        for k in range(count):
            passed = k < position
            running = combine(running, jax.tree.map(lambda part: part[k], pieces))
            inside = jax.tree.map(lambda new, old: jnp.where(passed, new, old), running, inside)
        before = combine(inside, before)
    return before


def block_masks(width):
    places = lax.broadcasted_iota(jnp.int32, (width, width), 0)
    others = lax.broadcasted_iota(jnp.int32, (width, width), 1)
    return (others < places, others <= places)


def pair_dots(left, right):
    return jnp.einsum("bhtn,bhsn->bhts", left, right, precision=highest)


def chain_product(first, second):
    return jnp.einsum("hij,hjk->hik", first, second, precision=highest)


def prepare_blocks(streams):
    recept, decay, key, value, unit, rate = streams
    width = recept.shape[2]
    size = recept.shape[3]
    strict, inclusive = block_masks(width)
    logs = jnp.log(decay)
    running = jnp.cumsum(logs, axis=2)
    through = jnp.exp(running)
    until = jnp.exp(running - logs)
    alpha = -unit * until
    beta = unit * rate / through
    key_scaled = key / through
    recept_scaled = recept * through
    lower_ab = jnp.where(strict, pair_dots(alpha, beta), 0.0)
    lower_ak = jnp.where(strict, pair_dots(alpha, key_scaled), 0.0)
    system = jnp.eye(width, dtype=jnp.float32) - lower_ab
    targets = jnp.concatenate(
        [alpha, jnp.einsum("bhts,bhsr->bhtr", lower_ak, value, precision=highest)], axis=3
    )
    solved = jax.scipy.linalg.solve_triangular(system, targets, lower=True, unit_diagonal=True)
    solved_alpha = solved[..., :size]
    solved_value = solved[..., size:]
    final = through[:, :, -1:, :]
    beta_final = beta * final
    key_final = key_scaled * final
    transition = jnp.eye(size, dtype=jnp.float32) * final + jnp.einsum(
        "bhtm,bhtn->bhmn", solved_alpha, beta_final, precision=highest
    )
    added = jnp.einsum("bhtr,bhtn->bhrn", solved_value, beta_final, precision=highest) + jnp.einsum(
        "bhtr,bhtn->bhrn", value, key_final, precision=highest
    )
    upper_b = jnp.where(inclusive, pair_dots(recept_scaled, beta), 0.0)
    upper_k = jnp.where(inclusive, pair_dots(recept_scaled, key_scaled), 0.0)
    reads = recept_scaled + jnp.einsum("bhts,bhsn->bhtn", upper_b, solved_alpha, precision=highest)
    fixed_out = jnp.einsum(
        "bhts,bhsr->bhtr", upper_b, solved_value, precision=highest
    ) + jnp.einsum("bhts,bhsr->bhtr", upper_k, value, precision=highest)
    return (transition, added, reads, fixed_out)


def run_blocks(start, prepared, extra_rows, with_output):
    transition, added, reads, fixed_out = prepared
    if extra_rows > 0:
        added = jnp.concatenate(
            [added, jnp.zeros(added.shape[:2] + (extra_rows, added.shape[3]), jnp.float32)], axis=2
        )
        fixed_out = jnp.concatenate(
            [fixed_out, jnp.zeros(fixed_out.shape[:3] + (extra_rows,), jnp.float32)], axis=3
        )

    def block_step(state, inputs):
        trans_now, added_now, reads_now, fixed_now = inputs
        new_state = jnp.einsum("hrm,hmn->hrn", state, trans_now, precision=highest) + added_now
        if with_output:
            readout = jnp.einsum("htn,hrn->htr", reads_now, state, precision=highest) + fixed_now
            return (new_state, readout)
        return (new_state, None)

    return lax.scan(block_step, start, (transition, added, reads, fixed_out))


def per_device(
    tokens,
    norm_gain,
    w_recept,
    w_key,
    w_value,
    w_decay,
    w_rate,
    w_gate,
    shift_mix,
    decay_base,
    rate_base,
    decay_drift,
    group_gain,
    initial_state,
    w_out,
):
    tok_float = tokens.astype(jnp.float32)
    normed = (
        tok_float
        * lax.rsqrt(jnp.mean(tok_float * tok_float, axis=-1, keepdims=True) + norm_floor)
        * norm_gain
    ).astype(jnp.bfloat16)
    weights = (w_recept, w_key, w_value, w_decay, w_rate, w_gate)
    piece = gathered_copies(normed, "tp", 0)
    projected = jnp.stack(
        [
            jnp.dot(piece, weight, preferred_element_type=jnp.float32).astype(jnp.bfloat16)
            for weight in weights
        ],
        axis=0,
    )
    edge_rows = projected[0:3, -1:, :]
    earlier_rows = shifted_2(edge_rows, SP, 1)
    current = projected[0:3].astype(jnp.float32)
    earlier = jnp.concatenate([earlier_rows.astype(jnp.float32), current[:, :-1]], axis=1)
    shifted = current + (earlier - current) * shift_mix[:, None, :]
    recept, key, value = (shifted[0], shifted[1], shifted[2])
    level = decay_base + projected[3].astype(jnp.float32) + decay_drift[:, None]
    decay = jnp.exp(-jnp.exp(-jax.nn.softplus(-level) - 0.5))
    rate = jax.nn.sigmoid(rate_base + projected[4].astype(jnp.float32))
    gate = jax.nn.sigmoid(projected[5].astype(jnp.float32))
    seq_rows, local_width = recept.shape
    local_heads = local_width // HEAD
    block_count = seq_rows // BLOCK

    def blocked(array):
        return array.reshape(block_count, BLOCK, local_heads, HEAD).transpose(0, 2, 1, 3)

    key_heads = key.reshape(seq_rows, local_heads, HEAD)
    unit = key_heads * lax.rsqrt(jnp.sum(key_heads * key_heads, axis=-1, keepdims=True) + 1.0)
    streams = (
        blocked(recept),
        blocked(decay),
        blocked(key),
        blocked(value),
        blocked(unit.reshape(seq_rows, local_width)),
        blocked(rate),
    )
    prepared = prepare_blocks(streams)
    identity = jnp.broadcast_to(jnp.eye(HEAD, dtype=jnp.float32), (local_heads, HEAD, HEAD))
    empty = jnp.zeros((local_heads, HEAD, HEAD), jnp.float32)
    start_state = jnp.concatenate([empty, identity], axis=1)

    def combine(earlier_pair, later_pair):
        first_map, first_add = earlier_pair
        second_map, second_add = later_pair
        return (
            chain_product(first_map, second_map),
            chain_product(first_add, second_map) + second_add,
        )

    stretch, _ = run_blocks(start_state, prepared, HEAD, False)
    prefix_map, prefix_add = carried_in(
        (stretch[:, HEAD:], stretch[:, :HEAD]), SP, combine, (identity, empty)
    )
    carried = chain_product(initial_state, prefix_map) + prefix_add
    _, mixed = run_blocks(carried, prepared, 0, True)
    center = mixed - jnp.mean(mixed, axis=-1, keepdims=True)
    spread = jnp.mean(center * center, axis=-1, keepdims=True)
    gains = group_gain.reshape(local_heads, HEAD)[None, :, None, :]
    scaled = center * lax.rsqrt(spread + group_floor) * gains
    flat = scaled.transpose(0, 2, 1, 3).reshape(seq_rows, local_width)
    gated = (flat * gate).astype(jnp.bfloat16)
    token_rows = lax.all_to_all(gated, "tp", split_axis=0, concat_axis=1, tiled=True)
    result = jnp.dot(token_rows, w_out, preferred_element_type=jnp.float32).astype(jnp.bfloat16)
    return result


def solution(mesh):
    finer = Mesh(mesh.devices.reshape(8, 4, 2, mesh.shape["tp"]), ("sp_0", "sp_1", "sp_2", "tp"))
    in_specs = (
        P(SP_TP, None),
        P(),
        P(None, "tp"),
        P(None, "tp"),
        P(None, "tp"),
        P(None, "tp"),
        P(None, "tp"),
        P(None, "tp"),
        P(None, "tp"),
        P("tp"),
        P("tp"),
        P(SP),
        P("tp"),
        P("tp", None, None),
        P(),
    )
    out_specs = P(SP_TP, None)
    return jax.shard_map(
        per_device, mesh=finer, in_specs=in_specs, out_specs=out_specs, check_vma=False
    )
```

profile of v0, /device:TPU:32, one launch (start us, length us, event | category | flops | bytes accessed | tf_op | source)
XLA Modules:
  0.0 337.7 jit_solution(3600891156460394244)
XLA Ops:
  3.8 4.6 %all-to-all-start = ((bf16[4,96,2048]{2,1,0:T(8,128)(2,1)}), bf16[4,96,2048]{2,1,0:T(8,128)(2,1)S(1)}, u32[]{:S(2)}, u32[]{:S(2)}) async-start(bf16[4,96,2048]{2,1,0:T(8,128)(2,1)} %broadcast_in_dim.64), calls=%async_computation | async-start | bytes 3145728 | tf_op jit(solution)/shard_map/all_to_all | solution.py:20
  10.6 18.5 %all-to-all-done = bf16[4,96,2048]{2,1,0:T(8,128)(2,1)S(1)} async-done(((bf16[4,96,2048]{2,1,0:T(8,128)(2,1)}), bf16[4,96,2048]{2,1,0:T(8,128)(2,1)S(1)}, u32[]{:S(2)}, u32[]{:S(2)}) %all-to-all-start) | async-done | bytes 1572896 | tf_op jit(solution)/shard_map/all_to_all | solution.py:20
  34.1 2.5 collective-permute-start
  38.9 2.2 reshape.70
  46.5 2.2 reshape_squeeze.10
  48.7 2.8 bitcast_divide_fusion.1
  51.5 2.4 convolution_select_fusion
  53.9 2.3 convolution_select_fusion.1
  56.2 2.4 convolution_select_fusion.2
  58.6 2.3 fusion.16
  60.9 119.5 %custom-call.4 = f32[6,4,1,64,64]{3,4,2,1,0:T(8,128)} custom-call(f32[6,4,1,64,64]{4,3,2,1,0:T(8,128)} %fusion.16), custom_call_target="InvertDiagBlocksLowerTriangular" | custom-call | tf_op jit(solution)/shard_map/jit(_solve_triangular)/vmap(vmap())/triangular_solve | solution.py:96
  181.7 2.2 fusion.51
  187.5 1.9 fusion.55
  191.9 2.3 convolution_add_fusion.4
  198.1 7.2 %while.24 = (s32[]{:T(128)}, f32[4,128,64]{1,2,0:T(8,128)S(1)}, f32[6,4,64,64]{2,3,1,0:T(8,128)S(1)}, f32[6,4,128,64]{2,3,1,0:T(8,128)}) while((s32[]{:T(128)}, f32[4,128,64]{1,2,0:T(8,128)S(1)}, f32[6,4,64,64]{2,3,1,0:T(8,128)S(1)}, f32[6,4,128,64]{2,3,1,0:T(8,128)}) %tuple.52), condition=%wide.region_4.5_spmd.clone, body=%wide.region_3.4_spmd.sunk.clone | while | flops 25198592 | bytes 787517 | solution.py:135
  207.3 3.2 all-gather
  211.8 2.0 all-gather.3
  214.3 13.4 %all-gather.1 = f32[16,64,64]{2,1,0:T(8,128)S(1)} all-gather(f32[4,64,64]{2,1,0:T(8,128)S(1)} %fusion.125), channel_id=3, replica_groups=mesh['sp_0'=8,'sp_1'=4,'sp_2'=2,'tp'=4] {'sp_1'}, dimensions={0}, use_global_device_ids=true | all-gather | bytes 327680 | tf_op jit(solution)/shard_map/all_gather | solution.py:53
  228.7 13.6 %all-gather.4 = f32[16,64,64]{2,1,0:T(8,128)S(1)} all-gather(f32[4,64,64]{2,1,0:T(8,128)S(1)} %convolution_add_fusion.16), channel_id=6, replica_groups=mesh['sp_0'=8,'sp_1'=4,'sp_2'=2,'tp'=4] {'sp_1'}, dimensions={0}, use_global_device_ids=true | all-gather | bytes 327680 | tf_op jit(solution)/shard_map/all_gather | solution.py:53
  243.3 28.7 %all-gather.2 = f32[32,64,64]{2,1,0:T(8,128)S(1)} all-gather(f32[4,64,64]{2,1,0:T(8,128)S(1)} %fusion.113), channel_id=4, replica_groups=mesh['sp_0'=8,'sp_1'=4,'sp_2'=2,'tp'=4] {'sp_0'}, dimensions={0}, use_global_device_ids=true | all-gather | bytes 589824 | tf_op jit(solution)/shard_map/all_gather | solution.py:53
  273.0 26.7 %all-gather.5 = f32[32,64,64]{2,1,0:T(8,128)S(1)} all-gather(f32[4,64,64]{2,1,0:T(8,128)S(1)} %convolution_add_fusion.13), channel_id=7, replica_groups=mesh['sp_0'=8,'sp_1'=4,'sp_2'=2,'tp'=4] {'sp_0'}, dimensions={0}, use_global_device_ids=true | all-gather | bytes 589824 | tf_op jit(solution)/shard_map/all_gather | solution.py:53
  307.4 14.6 %while.25 = (s32[]{:T(128)}, f32[4,64,64]{1,2,0:T(8,128)S(1)}, f32[6,4,64,64]{3,2,1,0:T(8,128)S(1)}, f32[6,4,64,64]{2,3,1,0:T(8,128)}, f32[6,4,64,64]{2,3,1,0:T(...) while((s32[]{:T(128)}, f32[4,64,64]{1,2,0:T(8,128)S(1)}, ...), condition=%wide.region_6.7_spmd.clone, body=%wide.region_5.6_spmd.sunk.clone | while | flops 25198592 | bytes 985173 | solution.py:135
  325.2 2.1 fusion.25
  327.2 8.7 %all_to_all.24 = bf16[4,96,256]{2,1,0:T(8,128)(2,1)S(1)} all-to-all(bf16[4,96,256]{2,1,0:T(8,128)(2,1)S(1)} %bitcast.188), channel_id=1, replica_groups=mesh['sp_0'=8,'sp_1'=4,'sp_2'=2,'tp'=4] {'tp'}, dimensions={0} | all-to-all | bytes 393216 | tf_op jit(solution)/shard_map/all_to_all | solution.py:222
  (192 shorter events, 69.8 us)
Async XLA Ops:
  0.0 29.1 %copy-start = (bf16[2048,256]{1,0:T(8,128)(2,1)S(1)}, bf16[2048,256]{1,0:T(8,128)(2,1)}, u32[]{:S(2)}) copy-start(bf16[2048,256]{1,0:T(8,128)(2,1)} %param.23) | copy-start | bytes 3145732
  3.8 4.6 %copy-start.29 = (f32[256]{0:T(256)S(1)}, f32[256]{0:T(256)}, u32[]{:S(2)}) copy-start(f32[256]{0:T(256)} %param.31) | copy-start | bytes 3076
  3.8 25.3 %all-to-all-start = ((bf16[4,96,2048]{2,1,0:T(8,128)(2,1)}), bf16[4,96,2048]{2,1,0:T(8,128)(2,1)S(1)}, u32[]{:S(2)}, u32[]{:S(2)}) async-start(bf16[4,96,2048]{2,1,0:T(8,128)(2,1)} %broadcast_in_dim.64), calls=%async_computation | async-start | bytes 3145728 | tf_op jit(solution)/shard_map/all_to_all | solution.py:20
  9.1 20.6 %copy-start.10 = (f32[64,64]{1,0:T(8,128)}, f32[64,64]{1,0:T(8,128)S(1)}, u32[]{:S(2)}) copy-start(f32[64,64]{1,0:T(8,128)S(1)} %get-tuple-element.134) | copy-start | bytes 49156
  29.1 8.4 %copy-start.16 = (bf16[4,96,2048]{2,1,0:T(8,128)(2,1)}, bf16[4,96,2048]{2,1,0:T(8,128)(2,1)S(1)}, u32[]{:S(2)}) copy-start(bf16[4,96,2048]{2,1,0:T(8,128)(2,1)S(1)} %all-to-all-done) | copy-start | bytes 4718596
  32.9 4.6 %copy-start.20 = (bf16[1,384,256]{2,1,0:T(8,128)(2,1)}, bf16[1,384,256]{2,1,0:T(8,128)(2,1)S(1)}, u32[]{:S(2)}) copy-start(bf16[1,384,256]{2,1,0:T(8,128)(2,1)S(1)} %fusion.36) | copy-start | bytes 589828
  32.9 3.7 %copy-start.32 = (bf16[2048,256]{1,0:T(8,128)(2,1)S(1)}, bf16[2048,256]{1,0:T(8,128)(2,1)}, u32[]{:S(2)}) copy-start(bf16[2048,256]{1,0:T(8,128)(2,1)} %param.24) | copy-start | bytes 3145732
  32.9 3.7 %copy-start.34 = (f32[384]{0:T(512)S(1)}, f32[384]{0:T(512)}, u32[]{:S(2)}) copy-start(f32[384]{0:T(512)} %param.30) | copy-start | bytes 4612
  32.9 3.7 %copy-start.35 = (f32[256]{0:T(256)S(1)}, f32[256]{0:T(256)}, u32[]{:S(2)}) copy-start(f32[256]{0:T(256)} %param.28) | copy-start | bytes 3076
  34.1 3.5 %copy-start.33 = (bf16[2048,256]{1,0:T(8,128)(2,1)S(1)}, bf16[2048,256]{1,0:T(8,128)(2,1)}, u32[]{:S(2)}) copy-start(bf16[2048,256]{1,0:T(8,128)(2,1)} %param.25) | copy-start | bytes 3145732
  34.1 3.5 %copy-start.36 = (f32[256]{0:T(256)S(1)}, f32[256]{0:T(256)}, u32[]{:S(2)}) copy-start(f32[256]{0:T(256)} %param.29) | copy-start | bytes 3076
  34.1 8.2 %collective-permute-start = (bf16[3,1,256]{2,1,0:T(2,128)(2,1)S(1)}, bf16[3,1,256]{2,1,0:T(2,128)(2,1)S(1)}, u32[]{:S(2)}, u32[]{:S(2)}) collective-permute-start(bf16[3,1,256]{2,1,0:T(2,128)(2,1)S(1)} %slice.190), channel_id=1, source_target_pairs={{0,4},{4,8},{8,12},{12,16},{16,20},{20,24},{24,28},{28,32},{32,36}... | collective-permute-start | bytes 4616 | tf_op jit(solution)/shard_map/ppermute | solution.py:39
  48.7 2.8 copy-start.1
  48.7 2.8 copy-start.6
  48.7 2.8 copy-start.27
  51.5 7.2 %copy-start.4 = (f32[6,4,64,64]{3,2,1,0:T(8,128)}, f32[6,4,64,64]{3,2,1,0:T(8,128)S(1)}, u32[]{:S(2)}) copy-start(f32[6,4,64,64]{3,2,1,0:T(8,128)S(1)} %get-tuple-element.122) | copy-start | bytes 1179652
  56.2 2.4 copy-start.11
  56.2 2.4 copy-start.23
  56.2 2.4 copy-start.26
  189.3 2.5 copy-start.12
  205.3 9.0 %copy-start.9 = (f32[6,4,64,64]{2,3,1,0:T(8,128)}, f32[6,4,64,64]{2,3,1,0:T(8,128)S(1)}, u32[]{:S(2)}) copy-start(f32[6,4,64,64]{2,3,1,0:T(8,128)S(1)} %get-tuple-element.263) | copy-start | bytes 1179652
  207.3 20.4 %copy-start.13 = (f32[64,64]{1,0:T(8,128)S(1)}, f32[64,64]{1,0:T(8,128)}, u32[]{:S(2)}) copy-start(f32[64,64]{1,0:T(8,128)} %copy-done.10) | copy-start | bytes 49156
  304.8 2.6 copy-start.3
  325.2 10.8 %copy-start.14 = (bf16[1024,2048]{1,0:T(8,128)(2,1)S(1)}, bf16[1024,2048]{1,0:T(8,128)(2,1)}, u32[]{:S(2)}) copy-start(bf16[1024,2048]{1,0:T(8,128)(2,1)} %param.33) | copy-start | bytes 12582916
  (15 other events, 25.6 us)
where the time goes:
time: 342 us; the launch traced here: 338 us
  other arithmetic  132 us (39%)
  blocking collectives  96.3 us (28%)
  matrix products  63.4 us (19%)
  local copies, waits for them, and re-layouts  18.5 us (5%)
  waiting for transfers between devices  18.5 us (5%)
  starting transfers between devices  7.11 us (2%)
    another operation x2, other arithmetic, prepare_blocks(): jax.scipy.linalg.solve_triangular(system, targets, lower=True, unit_diago...  119 us
    all_gather x6, blocking collectives, carried_in(): pieces = jax.tree.map(lambda part: lax.all_gather(part, axis), running)  87.6 us
    all_to_all x1, waiting for transfers between devices, copy_for_each(): lax.all_to_all(jnp.broadcast_to(shard[None], (count, *shard.shape)), axis...  18.5 us
    dot_general x12, matrix products, block_step(): jnp.einsum('hrm,hmn->hrn', state, trans_now, precision=highest) + added_now  14 us
    dot_general x35, matrix products, chain_product(): return jnp.einsum('hij,hjk->hik', first, second, precision=highest)  10.3 us
    dot_general x4, matrix products, pair_dots(): return jnp.einsum('bhtn,bhsn->bhts', left, right, precision=highest)  9.39 us
    all_to_all x1, blocking collectives, per_device(): lax.all_to_all(gated, 'tp', split_axis=0, concat_axis=1, tiled=True)  8.69 us
    dot_general x6, matrix products, block_step(): jnp.einsum('htn,hrn->htr', reads_now, state, precision=highest) + fixed_now  7.37 us
  transfers between devices with their start and end apart: 2, of which 1 were waited for; matrix products, arithmetic and copies ran while one was open for 2% of the time, Pallas kernels for 0%

commit v1 on v0

v1 whole, which is shorter than its diff:
```python
import functools

import jax
import jax.numpy as jnp
from jax import lax
from jax.experimental import pallas as pl
from jax.experimental.pallas import tpu as pltpu
from jax.sharding import Mesh
from jax.sharding import PartitionSpec as P

HEAD = 64
BLOCK = 64
PAIR = 128
SP = ("z", "x", "c")
SP_TP = ("z", "x", "c", "tp")
AXES = ("z", "x", "c", "tp")
MESH = pl.DeviceIdType.MESH
NORM_FLOOR = 0.5
GROUP_FLOOR = 1.0
EXP_HALF = 0.6065306597126334
f32 = jnp.float32
bf16 = jnp.bfloat16
VMEM_SPEC = pl.BlockSpec(memory_space=pltpu.VMEM)
ANY_SPEC = pl.BlockSpec(memory_space=pl.ANY)
SMEM_SPEC = pl.BlockSpec(memory_space=pltpu.SMEM)


def here():
    return {axis: lax.axis_index(axis) for axis in AXES}


def split(x):
    hi = x.astype(bf16)
    lo = (x - hi.astype(f32)).astype(bf16)
    return hi, lo


def sigmoid(x):
    return 1.0 / (1.0 + jnp.exp(-x))


def gather_project(tokens, gain, wr, wk, wv, wd, wa, wg, proj, edge_out, own, held, last, last_in, wbuf, norm_buf,
                   own_sem, w_sem, send_sem, recv_sem, edge_send, edge_recv):
    me = here()
    y = me["tp"]
    ny = lax.axis_size("tp")
    nx, nc, nz = lax.axis_size("x"), lax.axis_size("c"), lax.axis_size("z")
    right, left = lax.rem(y + 1, ny), lax.rem(y + ny - 1, ny)
    seq = (me["z"] * nx + me["x"]) * nc + me["c"]
    total = nx * nc * nz

    def at(index, tp):
        return {"z": index // (nx * nc), "x": lax.rem(index // nc, nx), "c": lax.rem(index, nc), "tp": tp}

    rows = own.shape[0]
    half = rows // 2
    weights = (wr, wk, wv, wd, wa, wg)
    fetch = pltpu.make_async_copy(tokens, own, own_sem)
    fetch.start()
    w_copies = [pltpu.make_async_copy(w, wbuf.at[i], w_sem.at[i]) for i, w in enumerate(weights)]
    for copy in w_copies:
        copy.start()
    barrier = pltpu.get_barrier_semaphore()
    for peer in (left, right):
        pl.semaphore_signal(barrier, inc=1, device_id={"tp": peer}, device_id_type=MESH)

    sends_edge = jnp.logical_and(y == ny - 1, seq < total - 1)
    gets_edge = seq > 0

    @pl.when(gets_edge)
    def _():
        pl.semaphore_signal(barrier, inc=1, device_id=at(seq - 1, ny - 1), device_id_type=MESH)

    pl.semaphore_wait(barrier, 2 + 4 * sends_edge.astype(jnp.int32))
    fetch.wait()

    def part(h):
        return pl.ds(h * half, half)

    def hop(src, slot, h, to, sem):
        return pltpu.make_async_remote_copy(
            src_ref=src, dst_ref=held.at[slot, part(h)], send_sem=send_sem.at[sem], recv_sem=recv_sem.at[slot, h],
            device_id={"tp": to}, device_id_type=MESH)

    to_right = [hop(own.at[part(h)], 0, h, right, h) for h in (0, 1)]
    to_left = [hop(own.at[part(h)], 2, h, left, 2 + h) for h in (0, 1)]
    on_right = hop(held.at[0, part(0)], 1, 0, right, 4)
    on_left = hop(held.at[2, part(1)], 1, 1, left, 5)
    to_right[0].start()
    to_left[1].start()
    to_right[1].start()
    to_left[0].start()

    last[...] = own[rows - 16:rows, :].astype(f32)[15:16, :]
    edges = [pltpu.make_async_remote_copy(
        src_ref=last, dst_ref=last_in, send_sem=edge_send.at[k], recv_sem=edge_recv,
        device_id=at(lax.rem(seq + 1, total), k), device_id_type=MESH) for k in range(4)]

    @pl.when(sends_edge)
    def _():
        for copy in edges:
            copy.start()

    def normalize(x):
        return (x * lax.rsqrt(jnp.mean(x * x, axis=-1, keepdims=True) + NORM_FLOOR) * gain[...]).astype(bf16)

    def project(block, base, with_edge):
        norm_buf[0:rows, :] = normalize(block[...].astype(f32))
        count = rows + 16 if with_edge else rows
        for i in range(6):
            res = jnp.dot(norm_buf[0:count, :], wbuf[i], preferred_element_type=f32)
            proj[pl.ds(pl.multiple_of(base, 16), rows), 256 * i:256 * (i + 1)] = res[0:rows].astype(bf16)
            if with_edge and i < 3:
                edge_out[0:1, 256 * i:256 * (i + 1)] = res[rows:rows + 1].astype(bf16).astype(f32)

    for copy in w_copies:
        copy.wait()
    project(own, y * rows, False)
    to_right[0].wait_recv()
    on_right.start()
    to_left[1].wait_recv()
    on_left.start()
    to_right[1].wait_recv()
    project(held.at[0], left * rows, False)
    to_left[0].wait_recv()
    project(held.at[2], right * rows, False)

    @pl.when(gets_edge)
    def _():
        edges[0].wait_recv()

    @pl.when(jnp.logical_not(gets_edge))
    def _():
        last_in[...] = jnp.zeros_like(last_in)

    norm_buf[rows:rows + 16, :] = normalize(jnp.broadcast_to(last_in[...], (16, last_in.shape[1])))
    on_right.wait_recv()
    on_left.wait_recv()
    project(held.at[1], lax.rem(y + 2, ny) * rows, True)
    for copy in (*to_right, *to_left, on_right, on_left):
        copy.wait_send()

    @pl.when(sends_edge)
    def _():
        for copy in edges:
            copy.wait_send()


def call_gather(tokens, gain, weights):
    rows, depth = tokens.shape
    width = weights[0].shape[1]
    return pl.pallas_call(
        gather_project,
        out_shape=(jax.ShapeDtypeStruct((4 * rows, 6 * width), bf16), jax.ShapeDtypeStruct((8, 3 * width), f32)),
        in_specs=[ANY_SPEC, VMEM_SPEC] + [ANY_SPEC] * 6,
        out_specs=(VMEM_SPEC, VMEM_SPEC),
        scratch_shapes=[
            pltpu.VMEM((rows, depth), bf16),
            pltpu.VMEM((3, rows, depth), bf16),
            pltpu.VMEM((1, depth), f32),
            pltpu.VMEM((1, depth), f32),
            pltpu.VMEM((6, depth, width), bf16),
            pltpu.VMEM((rows + 16, depth), bf16),
            pltpu.SemaphoreType.DMA(()),
            pltpu.SemaphoreType.DMA((6,)),
            pltpu.SemaphoreType.DMA((6,)),
            pltpu.SemaphoreType.DMA((3, 2)),
            pltpu.SemaphoreType.DMA((4,)),
            pltpu.SemaphoreType.DMA(()),
        ],
        compiler_params=pltpu.CompilerParams(collective_id=0, has_side_effects=True),
        name="gather_project",
    )(tokens, gain, *weights)


def lane_masks(dtype):
    lane = lax.broadcasted_iota(jnp.int32, (1, PAIR), 1)
    low = (lane < HEAD).astype(f32)
    return low.astype(dtype), (1.0 - low).astype(dtype)


def lhs3(x):
    hi, lo = split(x)
    return jnp.concatenate([hi, lo, hi], axis=1)


def diag_parts(x, masks):
    hi, lo = split(x)
    low, high = masks
    bd_hi = jnp.concatenate([hi * low, hi * high], axis=0)
    bd_lo = jnp.concatenate([lo * low, lo * high], axis=0)
    return bd_hi, bd_lo


def rhs_nn(x, masks):
    hi, lo = diag_parts(x, masks)
    return jnp.concatenate([hi, hi, lo], axis=0)


def rhs_nt(x, masks):
    hi, lo = diag_parts(x, masks)
    return jnp.concatenate([hi, hi, lo], axis=1)


def nn(a3, b3):
    return jnp.dot(a3, b3, preferred_element_type=f32)


def nt(a3, b3):
    return lax.dot_general(a3, b3, (((1,), (1,)), ((), ())), preferred_element_type=f32)


def tn(a, b):
    a_hi, a_lo = split(a)
    b_hi, b_lo = split(b)
    return lax.dot_general(
        jnp.concatenate([a_hi, a_lo, a_hi], axis=0), jnp.concatenate([b_hi, b_hi, b_lo], axis=0),
        (((0,), (0,)), ((), ())), preferred_element_type=f32)


def head_sum(x, masks):
    low, high = masks
    ones = jnp.concatenate([jnp.broadcast_to(low, (HEAD, PAIR)), jnp.broadcast_to(high, (HEAD, PAIR))], axis=0)
    hi, lo = split(x)
    return jnp.dot(jnp.concatenate([hi, lo], axis=1), jnp.concatenate([ones, ones], axis=0), preferred_element_type=f32)


def prepare(proj, edge, mix, base, rate_base, drift, reads_out, fixed_out, gate_out, msg,
            recept_s, key_s, value_s, unit_s, rate_s, logs_s, reads_s, fixed_s, trans_s, added_s):
    rows = proj.shape[0]
    width = proj.shape[1] // 6
    pairs = width // PAIR
    chunks = rows // BLOCK
    masks = lane_masks(bf16)
    lane = lax.broadcasted_iota(jnp.int32, (1, PAIR), 1)
    is_low = lane < HEAD
    for j in range(pairs):
        cols = slice(j * PAIR, (j + 1) * PAIR)
        first = lax.broadcasted_iota(jnp.int32, (rows, PAIR), 0) == 0

        def raw(i):
            return proj[:, i * width + j * PAIR:i * width + (j + 1) * PAIR].astype(f32)

        def shifted(i):
            now = raw(i)
            before = jnp.where(first, edge[0:1, i * width + j * PAIR:i * width + (j + 1) * PAIR], pltpu.roll(now, 1, 0))
            return now + (before - now) * mix[i:i + 1, cols]

        recept_s[:, cols] = shifted(0)
        key = shifted(1)
        key_s[:, cols] = key
        value_s[:, cols] = shifted(2)
        unit_s[:, cols] = key * lax.rsqrt(head_sum(key * key, masks) + 1.0)
        rate_s[:, cols] = sigmoid(rate_base[:, cols] + raw(4))
        gate_out[:, cols] = sigmoid(raw(5))
        for c in range(chunks):
            block = slice(c * BLOCK, (c + 1) * BLOCK)
            level = base[:, cols] + raw(3)[block] + drift[0, c * BLOCK]
            logs_s[block, cols] = -EXP_HALF * sigmoid(level)

    place = lax.broadcasted_iota(jnp.int32, (BLOCK, PAIR), 0)
    other = lax.rem(lax.broadcasted_iota(jnp.int32, (BLOCK, PAIR), 1), BLOCK)
    strict = other < place
    inclusive = other <= place
    eye = (other == place).astype(f32)
    tri2 = inclusive.astype(f32).astype(bf16)

    def step(c, _):
        block = pl.ds(pl.multiple_of(c * BLOCK, BLOCK), BLOCK)
        for j in range(pairs):
            cols = slice(j * PAIR, (j + 1) * PAIR)
            logs = logs_s[block, cols]
            unit = unit_s[block, cols]
            key = key_s[block, cols]
            value = value_s[block, cols]
            run = jnp.dot(tri2, jnp.concatenate(split(logs), axis=0), preferred_element_type=f32)
            last = run[BLOCK - 1:BLOCK, :]
            inverse = jnp.exp(-run)
            to_end = jnp.exp(last - run)
            unit_rate = unit * rate_s[block, cols]
            alpha = -unit * jnp.exp(run - logs)
            scaled = recept_s[block, cols] * jnp.exp(run)
            left = lhs3(jnp.concatenate([alpha, scaled], axis=0))
            by_beta = nt(left, rhs_nt(unit_rate * inverse, masks))
            by_key = nt(left, rhs_nt(key * inverse, masks))
            lower = jnp.where(strict, by_beta[:BLOCK], 0.0)
            lower_ak = jnp.where(strict, by_key[:BLOCK], 0.0)
            upper_b = lhs3(jnp.where(inclusive, by_beta[BLOCK:], 0.0))
            upper_k = lhs3(jnp.where(inclusive, by_key[BLOCK:], 0.0))
            solved = eye + jnp.where(lax.div(place, 2) == lax.div(other, 2), lower, 0.0)
            size = 2
            while size < BLOCK:
                inside = jnp.logical_and(
                    lax.div(place, 2 * size) == lax.div(other, 2 * size),
                    lax.div(place, size) != lax.div(other, size))
                corner = jnp.where(inside, lower, 0.0)
                turned = nn(lhs3(solved), rhs_nn(corner, masks))
                solved = solved + nn(lhs3(turned), rhs_nn(solved, masks))
                size *= 2
            value3 = rhs_nn(value, masks)
            solved3 = lhs3(solved)
            solved_alpha = nn(solved3, rhs_nn(alpha, masks))
            pulled = nn(lhs3(lower_ak), value3)
            solved_value = nn(solved3, rhs_nn(pulled, masks))
            reads_s[block, cols] = scaled + nn(upper_b, rhs_nn(solved_alpha, masks))
            fixed_s[block, cols] = nn(upper_b, rhs_nn(solved_value, masks)) + nn(upper_k, value3)
            beta_end = unit_rate * to_end
            cross = tn(solved_alpha, beta_end)
            trans_s[block, cols] = jnp.where(is_low, cross[:BLOCK], cross[BLOCK:]) + eye * jnp.exp(last)
            cross = tn(jnp.concatenate([solved_value, value], axis=0), jnp.concatenate([beta_end, key * to_end], axis=0))
            added_s[block, cols] = jnp.where(is_low, cross[:BLOCK], cross[BLOCK:])
        return 0

    lax.fori_loop(0, chunks, step, 0)

    zero = jnp.zeros((BLOCK, PAIR), f32)
    for j in range(pairs):
        cols = slice(j * PAIR, (j + 1) * PAIR)
        both = jnp.concatenate([eye, zero], axis=0)
        for c in range(chunks):
            block = slice(c * BLOCK, (c + 1) * BLOCK)
            if c == 0:
                reads_out[block, cols] = reads_s[block, cols]
                fixed_out[block, cols] = fixed_s[block, cols]
                both = jnp.concatenate([trans_s[block, cols], added_s[block, cols]], axis=0)
                continue
            reads = lhs3(reads_s[block, cols])
            reads_out[block, cols] = nt(reads, rhs_nt(both[:BLOCK], masks))
            fixed_out[block, cols] = fixed_s[block, cols] + nt(reads, rhs_nt(both[BLOCK:], masks))
            both = nn(lhs3(both), rhs_nn(trans_s[block, cols], masks)) + jnp.concatenate(
                [zero, added_s[block, cols]], axis=0)
        for side in range(2):
            head = 2 * j + side
            packed = pack(both[:BLOCK], side)
            for q in range(2):
                msg[2 * head + q, 0:32, :] = packed
                msg[2 * head + q, 32:48, :] = pack(both[BLOCK + 32 * q:BLOCK + 32 * (q + 1)], side)


def pack(x, side):
    half = x.shape[0] // 2
    is_low = lax.broadcasted_iota(jnp.int32, (half, PAIR), 1) < HEAD
    top, bottom = x[:half], x[half:]
    if side == 0:
        return jnp.where(is_low, top, pltpu.roll(bottom, HEAD, 1))
    return jnp.where(is_low, pltpu.roll(top, HEAD, 1), bottom)


def unpack(x):
    is_low = lax.broadcasted_iota(jnp.int32, x.shape, 1) < HEAD
    return jnp.concatenate([jnp.where(is_low, x, 0.0), jnp.where(is_low, pltpu.roll(x, HEAD, 1), 0.0)], axis=0)


def call_prepare(proj, edge, mix, base, rate_base, drift):
    rows = proj.shape[0]
    width = proj.shape[1] // 6
    wide = jax.ShapeDtypeStruct((rows, width), f32)
    return pl.pallas_call(
        prepare,
        out_shape=(wide, wide, wide, jax.ShapeDtypeStruct((8, 48, PAIR), f32)),
        in_specs=[VMEM_SPEC] * 5 + [SMEM_SPEC],
        out_specs=(VMEM_SPEC,) * 4,
        scratch_shapes=[pltpu.VMEM((rows, width), f32)] * 10,
        name="prepare",
        cost_estimate=pl.CostEstimate(flops=3 * 10**9, bytes_accessed=4 * 10**6, transcendentals=10**6),
    )(proj, edge, mix, base, rate_base, drift)


def state_lhs(x):
    hi = x.astype(bf16).astype(f32)
    joined = hi + pltpu.roll(x - hi, HEAD, 1)
    return jnp.concatenate([joined.astype(bf16), hi.astype(bf16)], axis=1)


def state_rhs(x):
    hi, lo = split(x)
    return jnp.concatenate([hi, hi, lo, jnp.zeros_like(lo)], axis=0)


def carry(msg, start, out, slab, slab_sum, across, pre_map, pre_add, back,
          send1, recv1, send2, recv2, send3, recv3):
    me = here()
    nx, nc, nz = lax.axis_size("x"), lax.axis_size("c"), lax.axis_size("z")
    z = me["z"]
    unit = me["x"] * nc + me["c"]
    units = nx * nc

    def in_slab(index):
        return {"z": z, "x": index // nc, "c": lax.rem(index, nc), "tp": me["tp"]}

    def along(index):
        return {"z": index, "x": me["x"], "c": me["c"], "tp": me["tp"]}

    barrier = pltpu.get_barrier_semaphore()
    for d in range(1, units):
        pl.semaphore_signal(barrier, inc=1, device_id=in_slab(lax.rem(unit + d, units)), device_id_type=MESH)
    for d in range(1, nz):
        pl.semaphore_signal(barrier, inc=1, device_id=along(lax.rem(z + d, nz)), device_id_type=MESH)
    pl.semaphore_wait(barrier, units + nz - 2)

    first = []
    for d in range(1, units):
        peer = lax.rem(unit + d, units)
        copy = pltpu.make_async_remote_copy(
            src_ref=msg.at[peer], dst_ref=slab.at[unit], send_sem=send1.at[d], recv_sem=recv1.at[unit],
            device_id=in_slab(peer), device_id_type=MESH)
        copy.start()
        first.append(copy)
    slab[unit] = msg[unit]

    def landed(buffer, sems, k):
        return pltpu.make_async_remote_copy(
            src_ref=buffer.at[k], dst_ref=buffer.at[k], send_sem=send1.at[0], recv_sem=sems.at[k],
            device_id=in_slab(unit), device_id_type=MESH)

    running = jnp.zeros((96, PAIR), f32)
    row = lax.broadcasted_iota(jnp.int32, (96, PAIR), 0)
    col = lax.broadcasted_iota(jnp.int32, (96, PAIR), 1)
    running = (row == col).astype(f32) * (col < HEAD).astype(f32)
    for k in range(8):
        @pl.when(k != unit)
        def _():
            landed(slab, recv1, k).wait_recv()

        pre_map[k] = state_rhs(running[:HEAD])
        pre_add[k] = running[HEAD:]
        piece = slab[k]
        add = jnp.concatenate([jnp.zeros((HEAD, PAIR), f32), unpack(piece[32:48])], axis=0)
        running = nn(state_lhs(running), state_rhs(unpack(piece[0:32]))) + add
    slab_sum[0:32, :] = pack(running[:HEAD], 0)
    slab_sum[32:48, :] = pack(running[HEAD:], 0)

    def onward(d):
        return pltpu.make_async_remote_copy(
            src_ref=slab_sum, dst_ref=across.at[z], send_sem=send2.at[d], recv_sem=recv2.at[z],
            device_id=along(lax.rem(z + d, nz)), device_id_type=MESH)

    for d in range(1, 8):
        @pl.when(z + d < nz)
        def _():
            onward(d).start()

    head = start[me["x"], pl.ds(pl.multiple_of(me["c"] * 32, 32), 32), :]
    state = jnp.concatenate([head, jnp.zeros((32, PAIR - HEAD), f32)], axis=1)
    for k in range(7):
        @pl.when(k < z)
        def _():
            landed(across, recv2, k).wait_recv()

        piece = across[k]
        new = nn(state_lhs(state), state_rhs(unpack(piece[0:32]))) + unpack(piece[32:48])
        state = jnp.where(k < z, new, state)

    state3 = state_lhs(state)
    for k in range(8):
        back[k] = pack(nn(state3, pre_map[k]) + pre_add[k], 0)
    last = []
    for d in range(1, units):
        peer = lax.rem(unit + d, units)
        copy = pltpu.make_async_remote_copy(
            src_ref=back.at[peer], dst_ref=out.at[unit], send_sem=send3.at[d], recv_sem=recv3.at[unit],
            device_id=in_slab(peer), device_id_type=MESH)
        copy.start()
        last.append(copy)
    out[unit] = back[unit]
    for k in range(8):
        @pl.when(k != unit)
        def _():
            landed(out, recv3, k).wait_recv()
    for copy in first + last:
        copy.wait_send()
    for d in range(1, 8):
        @pl.when(z + d < nz)
        def _():
            onward(d).wait_send()


def call_carry(msg, start):
    return pl.pallas_call(
        carry,
        out_shape=jax.ShapeDtypeStruct((8, 16, PAIR), f32),
        in_specs=[VMEM_SPEC, VMEM_SPEC],
        out_specs=VMEM_SPEC,
        scratch_shapes=[
            pltpu.VMEM((8, 48, PAIR), f32),
            pltpu.VMEM((48, PAIR), f32),
            pltpu.VMEM((8, 48, PAIR), f32),
            pltpu.VMEM((8, 256, PAIR), bf16),
            pltpu.VMEM((8, 32, PAIR), f32),
            pltpu.VMEM((8, 16, PAIR), f32),
        ] + [pltpu.SemaphoreType.DMA((8,))] * 6,
        compiler_params=pltpu.CompilerParams(collective_id=1, has_side_effects=True),
        name="carry",
    )(msg, start)


def finish(reads, fixed, gate, state, gains, w_out, out, gated, token_rows, wbuf, w_sem, send_sem, recv_sem):
    me = here()
    y = me["tp"]
    ny = lax.axis_size("tp")
    fetch = pltpu.make_async_copy(w_out, wbuf, w_sem)
    fetch.start()
    barrier = pltpu.get_barrier_semaphore()
    for d in range(1, 4):
        pl.semaphore_signal(barrier, inc=1, device_id={"tp": lax.rem(y + d, ny)}, device_id_type=MESH)
    rows, width = reads.shape
    share = rows // 4
    masks = lane_masks(bf16)
    is_low = lax.broadcasted_iota(jnp.int32, (16, PAIR), 1) < HEAD
    for j in range(width // PAIR):
        cols = slice(j * PAIR, (j + 1) * PAIR)
        parts = []
        for q in range(2):
            a, b = state[4 * j + q], state[4 * j + 2 + q]
            parts.append(jnp.where(is_low, a, pltpu.roll(b, HEAD, 1)))
            parts.append(jnp.where(is_low, pltpu.roll(a, HEAD, 1), b))
        entering = jnp.concatenate(parts, axis=0)
        mixed = fixed[:, cols] + nt(lhs3(reads[:, cols]), rhs_nt(entering, masks))
        center = mixed - head_sum(mixed, masks) * (1.0 / HEAD)
        spread = head_sum(center * center, masks) * (1.0 / HEAD)
        scaled = center * lax.rsqrt(spread + GROUP_FLOOR) * gains[:, cols]
        gated[:, cols] = (scaled * gate[:, cols]).astype(bf16)
    pl.semaphore_wait(barrier, 3)

    def part(k):
        return pl.ds(pl.multiple_of(k * share, 16), share)

    copies = []
    for d in range(1, 4):
        peer = lax.rem(y + d, ny)
        copy = pltpu.make_async_remote_copy(
            src_ref=gated.at[part(peer)], dst_ref=token_rows.at[d], send_sem=send_sem.at[d], recv_sem=recv_sem.at[d],
            device_id={"tp": peer}, device_id_type=MESH)
        copy.start()
        copies.append(copy)
    fetch.wait()
    token_rows[0] = gated[part(y), :]
    for d in range(1, 4):
        copies[d - 1].wait_recv()
    total = jnp.zeros(out.shape, f32)
    for d in range(4):
        owner = lax.rem(y + ny - d, ny)
        total = total + jnp.dot(token_rows[d], wbuf[pl.ds(pl.multiple_of(owner * width, width), width), :],
                                preferred_element_type=f32)
    out[...] = total.astype(bf16)
    for copy in copies:
        copy.wait_send()


def call_finish(reads, fixed, gate, state, gains, w_out):
    rows, width = reads.shape
    share = rows // 4
    inner, depth = w_out.shape
    return pl.pallas_call(
        finish,
        out_shape=jax.ShapeDtypeStruct((share, depth), bf16),
        in_specs=[VMEM_SPEC] * 5 + [ANY_SPEC],
        out_specs=VMEM_SPEC,
        scratch_shapes=[
            pltpu.VMEM((rows, width), bf16),
            pltpu.VMEM((4, share, width), bf16),
            pltpu.VMEM((inner, depth), bf16),
            pltpu.SemaphoreType.DMA(()),
            pltpu.SemaphoreType.DMA((4,)),
            pltpu.SemaphoreType.DMA((4,)),
        ],
        compiler_params=pltpu.CompilerParams(collective_id=2, has_side_effects=True),
        name="finish",
    )(reads, fixed, gate, state, gains, w_out)


def per_device(tokens, norm_gain, w_recept, w_key, w_value, w_decay, w_rate, w_gate, shift_mix, decay_base, rate_base,
               decay_drift, group_gain, initial_state, w_out):
    proj, edge = call_gather(
        tokens, norm_gain.reshape(1, -1), (w_recept, w_key, w_value, w_decay, w_rate, w_gate))
    reads, fixed, gate, msg = call_prepare(
        proj, edge, shift_mix, decay_base.reshape(1, -1), rate_base.reshape(1, -1), decay_drift.reshape(1, -1))
    state = call_carry(msg, initial_state)
    return call_finish(reads, fixed, gate, state, group_gain.reshape(1, -1), w_out)


def solution(mesh):
    finer = Mesh(mesh.devices.reshape(8, 4, 2, mesh.shape["tp"]), AXES)
    in_specs = (
        P(SP_TP, None),
        P(),
        P(None, "tp"),
        P(None, "tp"),
        P(None, "tp"),
        P(None, "tp"),
        P(None, "tp"),
        P(None, "tp"),
        P(None, "tp"),
        P("tp"),
        P("tp"),
        P(SP),
        P("tp"),
        P("tp", None, None),
        P(),
    )
    return jax.shard_map(
        per_device, mesh=finer, in_specs=in_specs, out_specs=P(SP_TP, None), check_vma=False
    )
```

time: 342 us -> 88.8 us (0.26)
  other arithmetic: 132 us -> 0 us
  blocking collectives: 96.3 us -> 0 us
  Pallas kernels: 0 us -> 84.2 us
  matrix products: 63.4 us -> 0 us
  waiting for transfers between devices: 18.5 us -> 0 us
  local copies, waits for them, and re-layouts: 18.5 us -> 3.04 us
  starting transfers between devices: 7.11 us -> 0 us
    another operation x4 -> x0, other arithmetic: 121 us -> none  [the longest x2 119 us: prepare_blocks(): jax.scipy.linalg.solve_triangular(system, targets, lower=True, unit_diago...]
    all_gather x6 -> x0, blocking collectives: 87.6 us -> none  [carried_in(): pieces = jax.tree.map(lambda part: lax.all_gather(part, axis), running)]
    pallas_call x0 -> x4, Pallas kernels: none -> 84.2 us  [the longest x1 29.8 us: call_prepare(): pl.pallas_call(prepare, out_shape=(wide, wide, wide, jax.ShapeDtypeStruct...]
    dot_general x71 -> x0, matrix products: 61.7 us -> none  [the longest x12 14 us: block_step(): jnp.einsum('hrm,hmn->hrn', state, trans_now, precision=highest) + added_now]
    all_to_all x1 -> x0, waiting for transfers between devices: 18.5 us -> none  [copy_for_each(): lax.all_to_all(jnp.broadcast_to(shard[None], (count, *shard.shape)), axis...]
    all_to_all x1 -> x0, blocking collectives: 8.69 us -> none  [per_device(): lax.all_to_all(gated, 'tp', split_axis=0, concat_axis=1, tiled=True)]
    another operation x3 -> x0, local copies, waits for them, and re-layouts: 4.77 us -> none  [the longest x2 2.56 us: blocked(): array.reshape(block_count, BLOCK, local_heads, HEAD).transpose(0, 2, 1, 3)]
    all_to_all x1 -> x0, starting transfers between devices: 4.59 us -> none  [copy_for_each(): lax.all_to_all(jnp.broadcast_to(shard[None], (count, *shard.shape)), axis...]
  transfers between devices with their start and end apart: 2 -> 0, of which waited for: 1 -> 0; matrix products, arithmetic and copies ran while one was open for 2% -> 0% of each run, Pallas kernels for 0% -> 0%
where the time goes in v1:
time: 88.8 us; the launch traced here: 87.3 us
  Pallas kernels  84.2 us (95%)
  local copies, waits for them, and re-layouts  3.04 us (3%)
    pallas_call x1, Pallas kernels, call_prepare(): pl.pallas_call(prepare, out_shape=(wide, wide, wide, jax.ShapeDtypeStruct...  29.8 us
    pallas_call x1, Pallas kernels, call_carry(): pl.pallas_call(carry, out_shape=jax.ShapeDtypeStruct((8, 16, PAIR), f32),...  22.9 us
    pallas_call x1, Pallas kernels, call_gather(): pl.pallas_call(gather_project, out_shape=(jax.ShapeDtypeStruct((4 * rows,...  22.2 us
    pallas_call x1, Pallas kernels, call_finish(): pl.pallas_call(finish, out_shape=jax.ShapeDtypeStruct((share, depth), bf1...  9.36 us

profile of v1, /device:TPU:32, one launch (start us, length us, event | category | flops | bytes accessed | tf_op | source)
XLA Modules:
  0.0 87.3 jit_solution(10357092742031565653)
XLA Ops:
  0.0 1.3 %reshape.18.drift = f32[1,384]{1,0:T(1,128)} reshape(f32[384]{0:T(512)} %param.26) | data formatting | bytes 3072 | tf_op jit(solution)/shard_map/reshape | solution.py:577
  1.3 22.2 %gather_project.1 = (bf16[384,1536]{1,0:T(8,128)(2,1)}, f32[8,768]{1,0:T(8,128)}) custom-call(bf16[96,2048]{1,0:T(8,128)(2,1)} %tokens.1, f32[1,2048]{1,0:T(1,128)} %bitcast.4, bf16[2048,256]{1,0:T(8,128)(2,1)} %wr.1, bf16[2048,256]{1,0:T(8,128)(2,1)} %wk.1, bf16[2048,256]{1,0:T(8,128)(2,1)} %wv.1, bf16[2048,256]{1,0:T(8,128)(2,1)} %wd.1, ...), custom_call_target="tpu_custom_call" | custom-call | tf_op jit(solution)/shard_map/gather_project/pallas_call | solution.py:152
  23.5 29.8 %prepare.1 = (f32[384,256]{1,0:T(8,128)}, f32[384,256]{1,0:T(8,128)}, f32[384,256]{1,0:T(8,128)}, f32[8,48,128]{2,1,0:T(8,128)}) custom-call(bf16[384,1536]{1,0:T(8,128)(2,1)} %get-tuple-element.11.proj, f32[8,768]{1,0:T(8,128)} %get-tuple-element.12.edge, f32[3,256]{1,0:T(4,128)} %mix.1, f32[1,256]{1,0:T(1,128)} %bitcast.6, f32[1,256]{1,0:T(1,128)} %bitcast.7, ...), custom_call_target="tpu_custom_call" | custom-call | flops 3000000000 | bytes 4000000 | tf_op jit(solution)/shard_map/prepare/pallas_call | solution.py:358
  53.2 22.9 %carry.1.state = f32[8,16,128]{2,1,0:T(8,128)} custom-call(f32[8,48,128]{2,1,0:T(8,128)} %get-tuple-element.16.msg, f32[4,64,64]{2,1,0:T(8,128)} %start.1), custom_call_target="tpu_custom_call" | custom-call | tf_op jit(solution)/shard_map/carry/pallas_call | solution.py:479
  76.1 9.4 %finish.1 = bf16[96,2048]{1,0:T(8,128)(2,1)} custom-call(f32[384,256]{1,0:T(8,128)} %get-tuple-element.13.reads, f32[384,256]{1,0:T(8,128)} %get-tuple-element.14.fixed, f32[384,256]{1,0:T(8,128)} %get-tuple-element.15.gate, f32[8,16,128]{2,1,0:T(8,128)} %carry.1.state, f32[1,256]{1,0:T(1,128)} %bitcast.5, bf16[1024,2048]{1,0:T(8,128)(2,1)} %w_out.1), custom_call_target="tpu_custom_call" | custom-call | tf_op jit(solution)/shard_map/finish/pallas_call | solution.py:554
  85.5 1.8 %copy.17 = bf16[96,2048]{1,0:T(8,128)(2,1)} copy(bf16[96,2048]{1,0:T(8,128)(2,1)} %finish.1) | data formatting | bytes 786432

commit v2 on v1

--- a/solution.py
+++ b/solution.py
@@ -11,6 +11,7 @@
 HEAD = 64
 BLOCK = 64
 PAIR = 128
+GROUP = 3
 SP = ("z", "x", "c")
 SP_TP = ("z", "x", "c", "tp")
 AXES = ("z", "x", "c", "tp")
@@ -225,116 +226,160 @@
     return jnp.dot(jnp.concatenate([hi, lo], axis=1), jnp.concatenate([ones, ones], axis=0), preferred_element_type=f32)
 
 
-def prepare(proj, edge, mix, base, rate_base, drift, reads_out, fixed_out, gate_out, msg,
-            recept_s, key_s, value_s, unit_s, rate_s, logs_s, reads_s, fixed_s, trans_s, added_s):
-    rows = proj.shape[0]
-    width = proj.shape[1] // 6
+def state_group(base, edge_row, proj, mix, decay_base, rate_base, drift, store):
+    recept_s, value_s, alpha_s, pulled_s, upper_b, upper_k, trans_s, added_s = store
+    width = recept_s.shape[1]
     pairs = width // PAIR
-    chunks = rows // BLOCK
+    rows = GROUP * BLOCK
     masks = lane_masks(bf16)
-    lane = lax.broadcasted_iota(jnp.int32, (1, PAIR), 1)
-    is_low = lane < HEAD
-    for j in range(pairs):
-        cols = slice(j * PAIR, (j + 1) * PAIR)
-        first = lax.broadcasted_iota(jnp.int32, (rows, PAIR), 0) == 0
-
-        def raw(i):
-            return proj[:, i * width + j * PAIR:i * width + (j + 1) * PAIR].astype(f32)
-
-        def shifted(i):
-            now = raw(i)
-            before = jnp.where(first, edge[0:1, i * width + j * PAIR:i * width + (j + 1) * PAIR], pltpu.roll(now, 1, 0))
-            return now + (before - now) * mix[i:i + 1, cols]
-
-        recept_s[:, cols] = shifted(0)
-        key = shifted(1)
-        key_s[:, cols] = key
-        value_s[:, cols] = shifted(2)
-        unit_s[:, cols] = key * lax.rsqrt(head_sum(key * key, masks) + 1.0)
-        rate_s[:, cols] = sigmoid(rate_base[:, cols] + raw(4))
-        gate_out[:, cols] = sigmoid(raw(5))
-        for c in range(chunks):
-            block = slice(c * BLOCK, (c + 1) * BLOCK)
-            level = base[:, cols] + raw(3)[block] + drift[0, c * BLOCK]
-            logs_s[block, cols] = -EXP_HALF * sigmoid(level)
-
+    is_low = lax.broadcasted_iota(jnp.int32, (1, PAIR), 1) < HEAD
     place = lax.broadcasted_iota(jnp.int32, (BLOCK, PAIR), 0)
     other = lax.rem(lax.broadcasted_iota(jnp.int32, (BLOCK, PAIR), 1), BLOCK)
     strict = other < place
     inclusive = other <= place
     eye = (other == place).astype(f32)
     tri2 = inclusive.astype(f32).astype(bf16)
-
-    def step(c, _):
-        block = pl.ds(pl.multiple_of(c * BLOCK, BLOCK), BLOCK)
+    area = pl.ds(pl.multiple_of(base, BLOCK), rows)
+    units = [(i, j) for i in range(GROUP) for j in range(pairs)]
+
+    def block(i):
+        return pl.ds(pl.multiple_of(base + i * BLOCK, BLOCK), BLOCK)
+
+    def cols(j):
+        return slice(j * PAIR, (j + 1) * PAIR)
+
+    logs, unit, rate, key, value, recept = {}, {}, {}, {}, {}, {}
+    first = lax.broadcasted_iota(jnp.int32, (rows, PAIR), 0) == 0
+    for j in range(pairs):
+        def raw(i):
+            return proj[area, i * width + j * PAIR:i * width + (j + 1) * PAIR].astype(f32)
+
+        def shifted(i):
+            now = raw(i)
+            before = jnp.where(first, edge_row(i, j), pltpu.roll(now, 1, 0))
+            return now + (before - now) * mix[i:i + 1, cols(j)]
+
+        key_all = shifted(1)
+        unit_all = key_all * lax.rsqrt(head_sum(key_all * key_all, masks) + 1.0)
+        rate_all = sigmoid(rate_base[:, cols(j)] + raw(4))
+        level_all = decay_base[:, cols(j)] + raw(3)
+        recept_all = shifted(0)
+        value_all = shifted(2)
+        for i in range(GROUP):
+            at = slice(i * BLOCK, (i + 1) * BLOCK)
+            u = (i, j)
+            key[u], unit[u], rate[u], value[u], recept[u] = key_all[at], unit_all[at], rate_all[at], value_all[at], recept_all[at]
+            logs[u] = -EXP_HALF * sigmoid(level_all[at] + drift[0, base + i * BLOCK])
+
+    run = {u: jnp.dot(tri2, jnp.concatenate(split(logs[u]), axis=0), preferred_element_type=f32) for u in units}
+    alpha, scaled, by = {}, {}, {}
+    beta_end, key_end = {}, {}
+    for u in units:
+        last = run[u][BLOCK - 1:BLOCK, :]
+        inverse = jnp.exp(-run[u])
+        to_end = jnp.exp(last - run[u])
+        unit_rate = unit[u] * rate[u]
+        alpha[u] = -unit[u] * jnp.exp(run[u] - logs[u])
+        scaled[u] = recept[u] * jnp.exp(run[u])
+        left = lhs3(jnp.concatenate([alpha[u], scaled[u]], axis=0))
+        right = jnp.concatenate([rhs_nt(unit_rate * inverse, masks), rhs_nt(key[u] * inverse, masks)], axis=0)
+        by[u] = nt(left, right)
+        beta_end[u] = unit_rate * to_end
+        key_end[u] = key[u] * to_end
+    lower = {u: jnp.where(strict, by[u][:BLOCK, :PAIR], 0.0) for u in units}
+    value3 = {u: rhs_nn(value[u], masks) for u in units}
+    pulled = {u: nn(lhs3(jnp.where(strict, by[u][:BLOCK, PAIR:], 0.0)), value3[u]) for u in units}
+    for u in units:
+        i, j = u
+        upper_b[block(i), cols(j)] = jnp.where(inclusive, by[u][BLOCK:, :PAIR], 0.0)
+        upper_k[block(i), cols(j)] = jnp.where(inclusive, by[u][BLOCK:, PAIR:], 0.0)
+        recept_s[block(i), cols(j)] = scaled[u]
+        value_s[block(i), cols(j)] = value[u]
+    solved = {u: eye + jnp.where(lax.div(place, 2) == lax.div(other, 2), lower[u], 0.0) for u in units}
+    size = 2
+    while size < BLOCK:
+        inside = jnp.logical_and(
+            lax.div(place, 2 * size) == lax.div(other, 2 * size), lax.div(place, size) != lax.div(other, size))
+        turned = {u: nn(lhs3(solved[u]), rhs_nn(jnp.where(inside, lower[u], 0.0), masks)) for u in units}
+        solved = {u: solved[u] + nn(lhs3(turned[u]), rhs_nn(solved[u], masks)) for u in units}
+        size *= 2
+    both = {u: nn(lhs3(solved[u]), jnp.concatenate([rhs_nn(alpha[u], masks), rhs_nn(pulled[u], masks)], axis=1))
+            for u in units}
+    for u in units:
+        i, j = u
+        alpha_s[block(i), cols(j)] = both[u][:, :PAIR]
+        pulled_s[block(i), cols(j)] = both[u][:, PAIR:]
+        cross = tn(both[u][:, :PAIR], beta_end[u])
+        trans_s[block(i), cols(j)] = jnp.where(is_low, cross[:BLOCK], cross[BLOCK:]) + eye * jnp.exp(run[u][BLOCK - 1:BLOCK, :])
+        cross = tn(jnp.concatenate([both[u][:, PAIR:], value[u]], axis=0),
+                   jnp.concatenate([beta_end[u], key_end[u]], axis=0))
+        added_s[block(i), cols(j)] = jnp.where(is_low, cross[:BLOCK], cross[BLOCK:])
+
+
+def compose(trans_s, added_s, before_s, msg):
+    width = trans_s.shape[1]
+    pairs = width // PAIR
+    chunks = trans_s.shape[0] // BLOCK
+    masks = lane_masks(bf16)
+    zero = jnp.zeros((BLOCK, PAIR), f32)
+    both = {}
+    for c in range(chunks):
+        block = slice(c * BLOCK, (c + 1) * BLOCK)
         for j in range(pairs):
             cols = slice(j * PAIR, (j + 1) * PAIR)
-            logs = logs_s[block, cols]
-            unit = unit_s[block, cols]
-            key = key_s[block, cols]
-            value = value_s[block, cols]
-            run = jnp.dot(tri2, jnp.concatenate(split(logs), axis=0), preferred_element_type=f32)
-            last = run[BLOCK - 1:BLOCK, :]
-            inverse = jnp.exp(-run)
-            to_end = jnp.exp(last - run)
-            unit_rate = unit * rate_s[block, cols]
-            alpha = -unit * jnp.exp(run - logs)
-            scaled = recept_s[block, cols] * jnp.exp(run)
-            left = lhs3(jnp.concatenate([alpha, scaled], axis=0))
-            by_beta = nt(left, rhs_nt(unit_rate * inverse, masks))
-            by_key = nt(left, rhs_nt(key * inverse, masks))
-            lower = jnp.where(strict, by_beta[:BLOCK], 0.0)
-            lower_ak = jnp.where(strict, by_key[:BLOCK], 0.0)
-            upper_b = lhs3(jnp.where(inclusive, by_beta[BLOCK:], 0.0))
-            upper_k = lhs3(jnp.where(inclusive, by_key[BLOCK:], 0.0))
-            solved = eye + jnp.where(lax.div(place, 2) == lax.div(other, 2), lower, 0.0)
-            size = 2
-            while size < BLOCK:
-                inside = jnp.logical_and(
-                    lax.div(place, 2 * size) == lax.div(other, 2 * size),
-                    lax.div(place, size) != lax.div(other, size))
-                corner = jnp.where(inside, lower, 0.0)
-                turned = nn(lhs3(solved), rhs_nn(corner, masks))
-                solved = solved + nn(lhs3(turned), rhs_nn(solved, masks))
-                size *= 2
-            value3 = rhs_nn(value, masks)
-            solved3 = lhs3(solved)
-            solved_alpha = nn(solved3, rhs_nn(alpha, masks))
-            pulled = nn(lhs3(lower_ak), value3)
-            solved_value = nn(solved3, rhs_nn(pulled, masks))
-            reads_s[block, cols] = scaled + nn(upper_b, rhs_nn(solved_alpha, masks))
-            fixed_s[block, cols] = nn(upper_b, rhs_nn(solved_value, masks)) + nn(upper_k, value3)
-            beta_end = unit_rate * to_end
-            cross = tn(solved_alpha, beta_end)
-            trans_s[block, cols] = jnp.where(is_low, cross[:BLOCK], cross[BLOCK:]) + eye * jnp.exp(last)
-            cross = tn(jnp.concatenate([solved_value, value], axis=0), jnp.concatenate([beta_end, key * to_end], axis=0))
-            added_s[block, cols] = jnp.where(is_low, cross[:BLOCK], cross[BLOCK:])
-        return 0
-
-    lax.fori_loop(0, chunks, step, 0)
-
-    zero = jnp.zeros((BLOCK, PAIR), f32)
+            if c == 0:
+                both[j] = jnp.concatenate([trans_s[block, cols], added_s[block, cols]], axis=0)
+                continue
+            before_s[c, :, cols] = both[j]
+            both[j] = nn(lhs3(both[j]), rhs_nn(trans_s[block, cols], masks)) + jnp.concatenate(
+                [zero, added_s[block, cols]], axis=0)
     for j in range(pairs):
-        cols = slice(j * PAIR, (j + 1) * PAIR)
-        both = jnp.concatenate([eye, zero], axis=0)
-        for c in range(chunks):
-            block = slice(c * BLOCK, (c + 1) * BLOCK)
-            if c == 0:
-                reads_out[block, cols] = reads_s[block, cols]
-                fixed_out[block, cols] = fixed_s[block, cols]
-                both = jnp.concatenate([trans_s[block, cols], added_s[block, cols]], axis=0)
-                continue
-            reads = lhs3(reads_s[block, cols])
-            reads_out[block, cols] = nt(reads, rhs_nt(both[:BLOCK], masks))
-            fixed_out[block, cols] = fixed_s[block, cols] + nt(reads, rhs_nt(both[BLOCK:], masks))
-            both = nn(lhs3(both), rhs_nn(trans_s[block, cols], masks)) + jnp.concatenate(
-                [zero, added_s[block, cols]], axis=0)
         for side in range(2):
             head = 2 * j + side
-            packed = pack(both[:BLOCK], side)
+            packed = pack(both[j][:BLOCK], side)
             for q in range(2):
                 msg[2 * head + q, 0:32, :] = packed
-                msg[2 * head + q, 32:48, :] = pack(both[BLOCK + 32 * q:BLOCK + 32 * (q + 1)], side)
+                msg[2 * head + q, 32:48, :] = pack(both[j][BLOCK + 32 * q:BLOCK + 32 * (q + 1)], side)
+
+
+def read_chunks(proj, store, before_s, reads_out, fixed_out, gate_out):
+    recept_s, value_s, alpha_s, pulled_s, upper_b, upper_k, trans_s, added_s = store
+    width = recept_s.shape[1]
+    pairs = width // PAIR
+    masks = lane_masks(bf16)
+    for c in range(recept_s.shape[0] // BLOCK):
+        block = slice(c * BLOCK, (c + 1) * BLOCK)
+        for j in range(pairs):
+            cols = slice(j * PAIR, (j + 1) * PAIR)
+            upper = lhs3(upper_b[block, cols])
+            both = nn(upper, jnp.concatenate(
+                [rhs_nn(alpha_s[block, cols], masks), rhs_nn(pulled_s[block, cols], masks)], axis=1))
+            reads = recept_s[block, cols] + both[:, :PAIR]
+            fixed = both[:, PAIR:] + nn(lhs3(upper_k[block, cols]), rhs_nn(value_s[block, cols], masks))
+            if c > 0:
+                both = nt(lhs3(reads), jnp.concatenate(
+                    [rhs_nt(before_s[c, :BLOCK, cols], masks), rhs_nt(before_s[c, BLOCK:, cols], masks)], axis=0))
+                reads = both[:, :PAIR]
+                fixed = fixed + both[:, PAIR:]
+            reads_out[block, cols] = reads
+            fixed_out[block, cols] = fixed
+            gate_out[block, cols] = sigmoid(proj[block, 5 * width + j * PAIR:5 * width + (j + 1) * PAIR].astype(f32))
+
+
+def prepare(proj, edge, mix, base, rate_base, drift, reads_out, fixed_out, gate_out, msg, before_s, *store):
+    rows = proj.shape[0]
+    width = proj.shape[1] // 6
+    group = GROUP * BLOCK
+    for g in range(rows // group):
+        def edge_row(i, j):
+            at = slice(i * width + j * PAIR, i * width + (j + 1) * PAIR)
+            if g == 0:
+                return edge[0:1, at]
+            return proj[g * group - 16:g * group, at].astype(f32)[15:16]
+
+        state_group(g * group, edge_row, proj, mix, base, rate_base, drift, store)
+    compose(store[6], store[7], before_s, msg)
+    read_chunks(proj, store, before_s, reads_out, fixed_out, gate_out)
 
 
 def pack(x, side):
@@ -360,7 +405,7 @@
         out_shape=(wide, wide, wide, jax.ShapeDtypeStruct((8, 48, PAIR), f32)),
         in_specs=[VMEM_SPEC] * 5 + [SMEM_SPEC],
         out_specs=(VMEM_SPEC,) * 4,
-        scratch_shapes=[pltpu.VMEM((rows, width), f32)] * 10,
+        scratch_shapes=[pltpu.VMEM((rows // BLOCK, 2 * BLOCK, width), f32)] + [pltpu.VMEM((rows, width), f32)] * 8,
         name="prepare",
         cost_estimate=pl.CostEstimate(flops=3 * 10**9, bytes_accessed=4 * 10**6, transcendentals=10**6),
     )(proj, edge, mix, base, rate_base, drift)

time: 88.8 us -> 68.4 us (0.77)
  the two profiles are of different devices: /device:TPU:32 before, /device:TPU:192 now
where the time goes in v2:
time: 68.4 us; the launch traced here: 68.1 us
  Pallas kernels  65.1 us (95%)
  local copies, waits for them, and re-layouts  3.04 us (4%)
    pallas_call x1, Pallas kernels, call_carry(): pl.pallas_call(carry, out_shape=jax.ShapeDtypeStruct((8, 16, PAIR), f32),...  24.2 us
    pallas_call x1, Pallas kernels, call_gather(): pl.pallas_call(gather_project, out_shape=(jax.ShapeDtypeStruct((4 * rows,...  22.2 us
    pallas_call x1, Pallas kernels, call_finish(): pl.pallas_call(finish, out_shape=jax.ShapeDtypeStruct((share, depth), bf1...  9.36 us
    pallas_call x1, Pallas kernels, call_prepare(): pl.pallas_call(prepare, out_shape=(wide, wide, wide, jax.ShapeDtypeStruct...  9.33 us
    unnamed x1, local copies, waits for them, and re-layouts  1.77 us

profile of v2, /device:TPU:192, one launch (start us, length us, event | category | flops | bytes accessed | tf_op | source)
XLA Modules:
  0.0 68.1 jit_solution(10386054928849415542)
XLA Ops:
  0.0 1.3 %reshape.18.drift = f32[1,384]{1,0:T(1,128)} reshape(f32[384]{0:T(512)} %param.26) | data formatting | bytes 3072 | tf_op jit(solution)/shard_map/reshape | solution.py:622
  1.3 22.2 %gather_project.1 = (bf16[384,1536]{1,0:T(8,128)(2,1)}, f32[8,768]{1,0:T(8,128)}) custom-call(bf16[96,2048]{1,0:T(8,128)(2,1)} %tokens.1, f32[1,2048]{1,0:T(1,128)} %bitcast.4, bf16[2048,256]{1,0:T(8,128)(2,1)} %wr.1, bf16[2048,256]{1,0:T(8,128)(2,1)} %wk.1, bf16[2048,256]{1,0:T(8,128)(2,1)} %wv.1, bf16[2048,256]{1,0:T(8,128)(2,1)} %wd.1, ...), custom_call_target="tpu_custom_call" | custom-call | tf_op jit(solution)/shard_map/gather_project/pallas_call | solution.py:153
  23.5 9.3 %prepare.1 = (f32[384,256]{1,0:T(8,128)}, f32[384,256]{1,0:T(8,128)}, f32[384,256]{1,0:T(8,128)}, f32[8,48,128]{2,1,0:T(8,128)}) custom-call(bf16[384,1536]{1,0:T(8,128)(2,1)} %get-tuple-element.11.proj, f32[8,768]{1,0:T(8,128)} %get-tuple-element.12.edge, f32[3,256]{1,0:T(4,128)} %mix.1, f32[1,256]{1,0:T(1,128)} %bitcast.6, f32[1,256]{1,0:T(1,128)} %bitcast.7, ...), custom_call_target="tpu_custom_call" | custom-call | flops 3000000000 | bytes 4000000 | tf_op jit(solution)/shard_map/prepare/pallas_call | solution.py:403
  32.8 24.2 %carry.1.state = f32[8,16,128]{2,1,0:T(8,128)} custom-call(f32[8,48,128]{2,1,0:T(8,128)} %get-tuple-element.16.msg, f32[4,64,64]{2,1,0:T(8,128)} %start.1), custom_call_target="tpu_custom_call" | custom-call | tf_op jit(solution)/shard_map/carry/pallas_call | solution.py:524
  57.0 9.4 %finish.1 = bf16[96,2048]{1,0:T(8,128)(2,1)} custom-call(f32[384,256]{1,0:T(8,128)} %get-tuple-element.13.reads, f32[384,256]{1,0:T(8,128)} %get-tuple-element.14.fixed, f32[384,256]{1,0:T(8,128)} %get-tuple-element.15.gate, f32[8,16,128]{2,1,0:T(8,128)} %carry.1.state, f32[1,256]{1,0:T(1,128)} %bitcast.5, bf16[1024,2048]{1,0:T(8,128)(2,1)} %w_out.1), custom_call_target="tpu_custom_call" | custom-call | tf_op jit(solution)/shard_map/finish/pallas_call | solution.py:599
  66.4 1.8 %copy.17 = bf16[96,2048]{1,0:T(8,128)(2,1)} copy(bf16[96,2048]{1,0:T(8,128)(2,1)} %finish.1) | data formatting | bytes 786432

commit v3 on v2

v3 whole, which is shorter than its diff:
```python
import functools

import jax
import jax.numpy as jnp
from jax import lax
from jax.experimental import pallas as pl
from jax.experimental.pallas import tpu as pltpu
from jax.sharding import Mesh
from jax.sharding import PartitionSpec as P

HEAD = 64
BLOCK = 64
PAIR = 128
GROUP = 3
SP = ("z", "x", "c")
SP_TP = ("z", "x", "c", "tp")
AXES = ("z", "x", "c", "tp")
MESH = pl.DeviceIdType.MESH
NORM_FLOOR = 0.5
GROUP_FLOOR = 1.0
EXP_HALF = 0.6065306597126334
f32 = jnp.float32
bf16 = jnp.bfloat16
VMEM_SPEC = pl.BlockSpec(memory_space=pltpu.VMEM)
ANY_SPEC = pl.BlockSpec(memory_space=pl.ANY)
SMEM_SPEC = pl.BlockSpec(memory_space=pltpu.SMEM)


def here():
    return {axis: lax.axis_index(axis) for axis in AXES}


def split(x):
    hi = x.astype(bf16)
    lo = (x - hi.astype(f32)).astype(bf16)
    return hi, lo


def sigmoid(x):
    return 1.0 / (1.0 + jnp.exp(-x))


def lane_masks(dtype):
    lane = lax.broadcasted_iota(jnp.int32, (1, PAIR), 1)
    low = (lane < HEAD).astype(f32)
    return low.astype(dtype), (1.0 - low).astype(dtype)


def lhs3(x):
    hi, lo = split(x)
    return jnp.concatenate([hi, lo, hi], axis=1)


def diag_parts(x, masks):
    hi, lo = split(x)
    low, high = masks
    bd_hi = jnp.concatenate([hi * low, hi * high], axis=0)
    bd_lo = jnp.concatenate([lo * low, lo * high], axis=0)
    return bd_hi, bd_lo


def rhs_nn(x, masks):
    hi, lo = diag_parts(x, masks)
    return jnp.concatenate([hi, hi, lo], axis=0)


def rhs_nt(x, masks):
    hi, lo = diag_parts(x, masks)
    return jnp.concatenate([hi, hi, lo], axis=1)


def nn(a3, b3):
    return jnp.dot(a3, b3, preferred_element_type=f32)


def nt(a3, b3):
    return lax.dot_general(a3, b3, (((1,), (1,)), ((), ())), preferred_element_type=f32)


def tn(a, b):
    a_hi, a_lo = split(a)
    b_hi, b_lo = split(b)
    return lax.dot_general(
        jnp.concatenate([a_hi, a_lo, a_hi], axis=0), jnp.concatenate([b_hi, b_hi, b_lo], axis=0),
        (((0,), (0,)), ((), ())), preferred_element_type=f32)


def head_sum(x, masks):
    low, high = masks
    ones = jnp.concatenate([jnp.broadcast_to(low, (HEAD, PAIR)), jnp.broadcast_to(high, (HEAD, PAIR))], axis=0)
    hi, lo = split(x)
    return jnp.dot(jnp.concatenate([hi, lo], axis=1), jnp.concatenate([ones, ones], axis=0), preferred_element_type=f32)


def state_group(base, edge_row, proj, mix, decay_base, rate_base, drift, store):
    recept_s, value_s, alpha_s, pulled_s, upper_b, upper_k, trans_s, added_s = store
    width = recept_s.shape[1]
    pairs = width // PAIR
    rows = GROUP * BLOCK
    masks = lane_masks(bf16)
    is_low = lax.broadcasted_iota(jnp.int32, (1, PAIR), 1) < HEAD
    place = lax.broadcasted_iota(jnp.int32, (BLOCK, PAIR), 0)
    other = lax.rem(lax.broadcasted_iota(jnp.int32, (BLOCK, PAIR), 1), BLOCK)
    strict = other < place
    inclusive = other <= place
    eye = (other == place).astype(f32)
    tri2 = inclusive.astype(f32).astype(bf16)
    area = pl.ds(pl.multiple_of(base, BLOCK), rows)
    units = [(i, j) for i in range(GROUP) for j in range(pairs)]

    def block(i):
        return pl.ds(pl.multiple_of(base + i * BLOCK, BLOCK), BLOCK)

    def cols(j):
        return slice(j * PAIR, (j + 1) * PAIR)

    logs, unit, rate, key, value, recept = {}, {}, {}, {}, {}, {}
    first = lax.broadcasted_iota(jnp.int32, (rows, PAIR), 0) == 0
    for j in range(pairs):
        def raw(i):
            return proj[area, i * width + j * PAIR:i * width + (j + 1) * PAIR].astype(f32)

        def shifted(i):
            now = raw(i)
            before = jnp.where(first, edge_row(i, j), pltpu.roll(now, 1, 0))
            return now + (before - now) * mix[i:i + 1, cols(j)]

        key_all = shifted(1)
        unit_all = key_all * lax.rsqrt(head_sum(key_all * key_all, masks) + 1.0)
        rate_all = sigmoid(rate_base[:, cols(j)] + raw(4))
        level_all = decay_base[:, cols(j)] + raw(3)
        recept_all = shifted(0)
        value_all = shifted(2)
        for i in range(GROUP):
            at = slice(i * BLOCK, (i + 1) * BLOCK)
            u = (i, j)
            key[u], unit[u], rate[u], value[u], recept[u] = key_all[at], unit_all[at], rate_all[at], value_all[at], recept_all[at]
            logs[u] = -EXP_HALF * sigmoid(level_all[at] + drift[base + i * BLOCK])

    run = {u: jnp.dot(tri2, jnp.concatenate(split(logs[u]), axis=0), preferred_element_type=f32) for u in units}
    alpha, scaled, by = {}, {}, {}
    beta_end, key_end = {}, {}
    for u in units:
        last = run[u][BLOCK - 1:BLOCK, :]
        inverse = jnp.exp(-run[u])
        to_end = jnp.exp(last - run[u])
        unit_rate = unit[u] * rate[u]
        alpha[u] = -unit[u] * jnp.exp(run[u] - logs[u])
        scaled[u] = recept[u] * jnp.exp(run[u])
        left = lhs3(jnp.concatenate([alpha[u], scaled[u]], axis=0))
        right = jnp.concatenate([rhs_nt(unit_rate * inverse, masks), rhs_nt(key[u] * inverse, masks)], axis=0)
        by[u] = nt(left, right)
        beta_end[u] = unit_rate * to_end
        key_end[u] = key[u] * to_end
    lower = {u: jnp.where(strict, by[u][:BLOCK, :PAIR], 0.0) for u in units}
    value3 = {u: rhs_nn(value[u], masks) for u in units}
    pulled = {u: nn(lhs3(jnp.where(strict, by[u][:BLOCK, PAIR:], 0.0)), value3[u]) for u in units}
    for u in units:
        i, j = u
        upper_b[block(i), cols(j)] = jnp.where(inclusive, by[u][BLOCK:, :PAIR], 0.0)
        upper_k[block(i), cols(j)] = jnp.where(inclusive, by[u][BLOCK:, PAIR:], 0.0)
        recept_s[block(i), cols(j)] = scaled[u]
        value_s[block(i), cols(j)] = value[u]
    solved = {u: eye + jnp.where(lax.div(place, 2) == lax.div(other, 2), lower[u], 0.0) for u in units}
    size = 2
    while size < BLOCK:
        inside = jnp.logical_and(
            lax.div(place, 2 * size) == lax.div(other, 2 * size), lax.div(place, size) != lax.div(other, size))
        turned = {u: nn(lhs3(solved[u]), rhs_nn(jnp.where(inside, lower[u], 0.0), masks)) for u in units}
        solved = {u: solved[u] + nn(lhs3(turned[u]), rhs_nn(solved[u], masks)) for u in units}
        size *= 2
    both = {u: nn(lhs3(solved[u]), jnp.concatenate([rhs_nn(alpha[u], masks), rhs_nn(pulled[u], masks)], axis=1))
            for u in units}
    for u in units:
        i, j = u
        alpha_s[block(i), cols(j)] = both[u][:, :PAIR]
        pulled_s[block(i), cols(j)] = both[u][:, PAIR:]
        cross = tn(both[u][:, :PAIR], beta_end[u])
        trans_s[block(i), cols(j)] = jnp.where(is_low, cross[:BLOCK], cross[BLOCK:]) + eye * jnp.exp(run[u][BLOCK - 1:BLOCK, :])
        cross = tn(jnp.concatenate([both[u][:, PAIR:], value[u]], axis=0),
                   jnp.concatenate([beta_end[u], key_end[u]], axis=0))
        added_s[block(i), cols(j)] = jnp.where(is_low, cross[:BLOCK], cross[BLOCK:])


def compose(trans_s, added_s, before_s, msg):
    width = trans_s.shape[1]
    pairs = width // PAIR
    chunks = trans_s.shape[0] // BLOCK
    masks = lane_masks(bf16)
    zero = jnp.zeros((BLOCK, PAIR), f32)
    both = {}
    for c in range(chunks):
        block = slice(c * BLOCK, (c + 1) * BLOCK)
        for j in range(pairs):
            cols = slice(j * PAIR, (j + 1) * PAIR)
            if c == 0:
                both[j] = jnp.concatenate([trans_s[block, cols], added_s[block, cols]], axis=0)
                continue
            before_s[c, :, cols] = both[j]
            both[j] = nn(lhs3(both[j]), rhs_nn(trans_s[block, cols], masks)) + jnp.concatenate(
                [zero, added_s[block, cols]], axis=0)
    for j in range(pairs):
        for side in range(2):
            head = 2 * j + side
            packed = pack(both[j][:BLOCK], side)
            for q in range(2):
                msg[2 * head + q, 0:32, :] = packed
                msg[2 * head + q, 32:48, :] = pack(both[j][BLOCK + 32 * q:BLOCK + 32 * (q + 1)], side)


def read_chunks(chunks, proj, store, before_s, reads_out, fixed_out, gate_out):
    recept_s, value_s, alpha_s, pulled_s, upper_b, upper_k, trans_s, added_s = store
    width = recept_s.shape[1]
    pairs = width // PAIR
    masks = lane_masks(bf16)
    for c in chunks:
        block = slice(c * BLOCK, (c + 1) * BLOCK)
        for j in range(pairs):
            cols = slice(j * PAIR, (j + 1) * PAIR)
            upper = lhs3(upper_b[block, cols])
            both = nn(upper, jnp.concatenate(
                [rhs_nn(alpha_s[block, cols], masks), rhs_nn(pulled_s[block, cols], masks)], axis=1))
            reads = recept_s[block, cols] + both[:, :PAIR]
            fixed = both[:, PAIR:] + nn(lhs3(upper_k[block, cols]), rhs_nn(value_s[block, cols], masks))
            if c > 0:
                both = nt(lhs3(reads), jnp.concatenate(
                    [rhs_nt(before_s[c, :BLOCK, cols], masks), rhs_nt(before_s[c, BLOCK:, cols], masks)], axis=0))
                reads = both[:, :PAIR]
                fixed = fixed + both[:, PAIR:]
            reads_out[block, cols] = reads
            fixed_out[block, cols] = fixed
            gate_out[block, cols] = sigmoid(proj[block, 5 * width + j * PAIR:5 * width + (j + 1) * PAIR].astype(f32))


def pack(x, side):
    half = x.shape[0] // 2
    is_low = lax.broadcasted_iota(jnp.int32, (half, PAIR), 1) < HEAD
    top, bottom = x[:half], x[half:]
    if side == 0:
        return jnp.where(is_low, top, pltpu.roll(bottom, HEAD, 1))
    return jnp.where(is_low, pltpu.roll(top, HEAD, 1), bottom)


def unpack(x):
    is_low = lax.broadcasted_iota(jnp.int32, x.shape, 1) < HEAD
    return jnp.concatenate([jnp.where(is_low, x, 0.0), jnp.where(is_low, pltpu.roll(x, HEAD, 1), 0.0)], axis=0)


def state_lhs(x):
    hi = x.astype(bf16).astype(f32)
    joined = hi + pltpu.roll(x - hi, HEAD, 1)
    return jnp.concatenate([joined.astype(bf16), hi.astype(bf16)], axis=1)


def state_rhs(x):
    hi, lo = split(x)
    return jnp.concatenate([hi, hi, lo, jnp.zeros_like(lo)], axis=0)


def layer(tokens, gain, wr, wk, wv, wd, wa, wg, mix, decay_base, rate_base, drift, group_gain, start, w_out, out,
          own, held, last, last_in, wbuf, norm_buf, proj, edge_s, before_s, msg, reads_s, fixed_s, gate_s,
          slab, slab_sum, across, pre_map, pre_add, back, entering, gated, token_rows, w_out_buf,
          own_sem, w_sem, out_sem, hop_send, hop_recv, edge_send, edge_recv,
          send1, recv1, send2, recv2, send3, recv3, send4, recv4, *store):
    me = here()
    y, z = me["tp"], me["z"]
    ny, nx, nc, nz = lax.axis_size("tp"), lax.axis_size("x"), lax.axis_size("c"), lax.axis_size("z")
    right, left = lax.rem(y + 1, ny), lax.rem(y + ny - 1, ny)
    far = lax.rem(y + 2, ny)
    unit = me["x"] * nc + me["c"]
    units = nx * nc
    seq = z * units + unit
    total = units * nz
    rows = own.shape[0]
    half = rows // 2
    width = wbuf.shape[2]

    def at(index, tp):
        return {"z": index // units, "x": lax.rem(index // nc, nx), "c": lax.rem(index, nc), "tp": tp}

    def in_slab(index):
        return {"z": z, "x": index // nc, "c": lax.rem(index, nc), "tp": y}

    def along(index):
        return {"z": index, "x": me["x"], "c": me["c"], "tp": y}

    def remote(src, dst, send, recv, to):
        return pltpu.make_async_remote_copy(
            src_ref=src, dst_ref=dst, send_sem=send, recv_sem=recv, device_id=to, device_id_type=MESH)

    def greet(to):
        pl.semaphore_signal(barrier, inc=1, device_id=to, device_id_type=MESH)

    fetch = pltpu.make_async_copy(tokens, own, own_sem)
    fetch.start()
    w_copies = [pltpu.make_async_copy(w, wbuf.at[i], w_sem.at[i]) for i, w in enumerate((wr, wk, wv, wd, wa, wg))]
    for copy in w_copies:
        copy.start()
    barrier = pltpu.get_barrier_semaphore()
    for d in range(1, 4):
        greet({"tp": lax.rem(y + d, ny)})
    for d in range(1, 8):
        greet(in_slab(lax.rem(unit + d, units)))
        greet(along(lax.rem(z + d, nz)))
    ends_stretch = jnp.logical_and(y == ny - 1, seq < total - 1)
    has_before = seq > 0

    @pl.when(has_before)
    def _():
        greet(at(seq - 1, ny - 1))

    pl.semaphore_wait(barrier, 17 + 4 * ends_stretch.astype(jnp.int32))
    fetch.wait()

    def part(h):
        return pl.ds(h * half, half)

    def hop(src, slot, h, to, sem):
        return remote(src, held.at[slot, part(h)], hop_send.at[sem], hop_recv.at[slot, h], {"tp": to})

    to_right = [hop(own.at[part(h)], 0, h, right, h) for h in (0, 1)]
    to_left = [hop(own.at[part(h)], 2, h, left, 2 + h) for h in (0, 1)]
    on_right = hop(held.at[0, part(0)], 1, 0, right, 4)
    on_left = hop(held.at[2, part(1)], 1, 1, left, 5)
    to_right[0].start()
    to_left[1].start()
    to_right[1].start()
    to_left[0].start()

    last[...] = own[rows - 16:rows, :].astype(f32)[15:16, :]
    edges = [remote(last, last_in.at[0], edge_send.at[k], edge_recv.at[0], at(lax.rem(seq + 1, total), k))
             for k in range(4)]
    inner = [remote(last, last_in.at[1], edge_send.at[4 + k], edge_recv.at[1], {"tp": 2 + k}) for k in range(2)]

    @pl.when(ends_stretch)
    def _():
        for copy in edges:
            copy.start()

    @pl.when(y == 1)
    def _():
        for copy in inner:
            copy.start()

    out_copy = pltpu.make_async_copy(w_out, w_out_buf, out_sem)
    out_copy.start()

    def normalize(x):
        return (x * lax.rsqrt(jnp.mean(x * x, axis=-1, keepdims=True) + NORM_FLOOR) * gain[...]).astype(bf16)

    def project(block, owner, with_edge):
        base = pl.multiple_of(owner * rows, 16)
        norm_buf[0:rows, :] = normalize(block[...].astype(f32))
        count = rows + 16 if with_edge else rows
        for i in range(6):
            res = jnp.dot(norm_buf[0:count, :], wbuf[i], preferred_element_type=f32)
            proj[pl.ds(base, rows), width * i:width * (i + 1)] = res[0:rows].astype(bf16)
            if with_edge and i < 3:
                edge_s[:, width * i:width * (i + 1)] = res[rows:].astype(bf16).astype(f32)

    for copy in w_copies:
        copy.wait()
    project(own, y, False)
    to_right[0].wait_recv()
    on_right.start()
    to_left[1].wait_recv()
    on_left.start()

    @pl.when(has_before)
    def _():
        edges[0].wait_recv()

    @pl.when(jnp.logical_not(has_before))
    def _():
        last_in[0] = jnp.zeros_like(last)

    @pl.when(y >= 2)
    def _():
        inner[0].wait_recv()

    @pl.when(y < 2)
    def _():
        last_in[1] = jnp.zeros_like(last)

    norm_buf[rows:, :] = jnp.concatenate(
        [jnp.broadcast_to(normalize(last_in[k]), (8, own.shape[1])) for k in range(2)], axis=0)
    to_right[1].wait_recv()
    project(held.at[0], left, True)
    to_left[0].wait_recv()
    project(held.at[2], right, False)

    group = GROUP * BLOCK
    early = y < 2

    def columns(i, j):
        return slice(i * width + j * PAIR, i * width + (j + 1) * PAIR)

    def first_edge(i, j):
        return jnp.where(early, edge_s[0:1, columns(i, j)], edge_s[8:9, columns(i, j)])

    def second_edge(i, j):
        return jnp.where(early, proj[group - 16:group, columns(i, j)].astype(f32)[15:16], edge_s[0:1, columns(i, j)])

    own_base = jnp.where(early, 0, group)
    state_group(own_base, first_edge, proj, mix, decay_base, rate_base, drift, store)
    on_right.wait_recv()
    on_left.wait_recv()
    project(held.at[1], far, False)
    state_group(group - own_base, second_edge, proj, mix, decay_base, rate_base, drift, store)
    compose(store[6], store[7], before_s, msg)

    def landed(buffer, sems, k):
        return remote(buffer.at[k], buffer.at[k], send1.at[0], sems.at[k], in_slab(unit))

    first = []
    for d in range(1, 8):
        peer = lax.rem(unit + d, units)
        first.append(remote(msg.at[peer], slab.at[unit], send1.at[d], recv1.at[unit], in_slab(peer)))
        first[-1].start()
    slab[unit] = msg[unit]
    read_chunks((0, 1), proj, store, before_s, reads_s, fixed_s, gate_s)

    row = lax.broadcasted_iota(jnp.int32, (96, PAIR), 0)
    col = lax.broadcasted_iota(jnp.int32, (96, PAIR), 1)
    running = (row == col).astype(f32) * (col < HEAD).astype(f32)
    for k in range(8):
        @pl.when(k != unit)
        def _():
            landed(slab, recv1, k).wait_recv()

    for k in range(8):
        pre_map[k] = state_rhs(running[:HEAD])
        pre_add[k] = running[HEAD:]
        piece = slab[k]
        add = jnp.concatenate([jnp.zeros((HEAD, PAIR), f32), unpack(piece[32:48])], axis=0)
        running = nn(state_lhs(running), state_rhs(unpack(piece[0:32]))) + add
    slab_sum[0:32, :] = pack(running[:HEAD], 0)
    slab_sum[32:48, :] = pack(running[HEAD:], 0)

    def onward(d):
        return remote(slab_sum, across.at[z], send2.at[d], recv2.at[z], along(lax.rem(z + d, nz)))

    for d in (4, 3, 2, 1, 5, 6, 7):
        @pl.when(z + d < nz)
        def _():
            onward(d).start()

    read_chunks((2, 3, 4, 5), proj, store, before_s, reads_s, fixed_s, gate_s)
    begin = start[me["x"], pl.ds(pl.multiple_of(me["c"] * 32, 32), 32), :]
    state = jnp.concatenate([begin, jnp.zeros((32, PAIR - HEAD), f32)], axis=1)
    for k in range(7):
        @pl.when(k < z)
        def _():
            landed(across, recv2, k).wait_recv()

    for k in range(7):
        piece = across[k]
        new = nn(state_lhs(state), state_rhs(unpack(piece[0:32]))) + unpack(piece[32:48])
        state = jnp.where(k < z, new, state)
    state3 = state_lhs(state)
    for k in range(8):
        back[k] = pack(nn(state3, pre_map[k]) + pre_add[k], 0)
    third = []
    for d in range(1, 8):
        peer = lax.rem(unit + d, units)
        third.append(remote(back.at[peer], entering.at[unit], send3.at[d], recv3.at[unit], in_slab(peer)))
        third[-1].start()
    entering[unit] = back[unit]
    for k in range(8):
        @pl.when(k != unit)
        def _():
            landed(entering, recv3, k).wait_recv()

    masks = lane_masks(bf16)
    is_low = lax.broadcasted_iota(jnp.int32, (16, PAIR), 1) < HEAD
    turned = []
    for j in range(width // PAIR):
        parts = []
        for q in range(2):
            a, b = entering[4 * j + q], entering[4 * j + 2 + q]
            parts.append(jnp.where(is_low, a, pltpu.roll(b, HEAD, 1)))
            parts.append(jnp.where(is_low, pltpu.roll(a, HEAD, 1), b))
        turned.append(rhs_nt(jnp.concatenate(parts, axis=0), masks))

    def share(k):
        return pl.ds(pl.multiple_of(k * rows, 16), rows)

    def gate_rows(at_rows):
        for j in range(width // PAIR):
            cols = slice(j * PAIR, (j + 1) * PAIR)
            mixed = fixed_s[at_rows, cols] + nt(lhs3(reads_s[at_rows, cols]), turned[j])
            center = mixed - head_sum(mixed, masks) * (1.0 / HEAD)
            spread = head_sum(center * center, masks) * (1.0 / HEAD)
            scaled = center * lax.rsqrt(spread + GROUP_FLOOR) * group_gain[:, cols]
            gated[at_rows, cols] = (scaled * gate_s[at_rows, cols]).astype(bf16)

    fourth = {}
    for d in (2, 1, 3):
        peer = lax.rem(y + d, ny)
        gate_rows(share(peer))
        fourth[d] = remote(gated.at[share(peer)], token_rows.at[d], send4.at[d], recv4.at[d], {"tp": peer})
    for d in (2, 1, 3):
        fourth[d].start()
    gate_rows(share(y))
    out_copy.wait()

    def product(block, owner):
        return jnp.dot(block, w_out_buf[pl.ds(pl.multiple_of(owner * width, width), width), :],
                       preferred_element_type=f32)

    result = product(gated[share(y), :], y)
    for d in (1, 3, 2):
        fourth[d].wait_recv()
        result = result + product(token_rows[d], lax.rem(y + ny - d, ny))
    out[...] = result.astype(bf16)

    for copy in (*to_right, *to_left, on_right, on_left, *first, *third, *fourth.values()):
        copy.wait_send()
    for d in range(1, 8):
        @pl.when(z + d < nz)
        def _():
            onward(d).wait_send()

    @pl.when(ends_stretch)
    def _():
        for copy in edges:
            copy.wait_send()

    @pl.when(y == 1)
    def _():
        for copy in inner:
            copy.wait_send()


def call_layer(tokens, gain, weights, mix, decay_base, rate_base, drift, group_gain, start, w_out):
    rows, depth = tokens.shape
    width = weights[0].shape[1]
    inner = w_out.shape[0]
    length = 4 * rows
    dma = pltpu.SemaphoreType.DMA
    return pl.pallas_call(
        layer,
        out_shape=jax.ShapeDtypeStruct((rows, depth), bf16),
        in_specs=[ANY_SPEC, VMEM_SPEC] + [ANY_SPEC] * 6 + [VMEM_SPEC] * 3 + [SMEM_SPEC] + [VMEM_SPEC] * 2 + [ANY_SPEC],
        out_specs=VMEM_SPEC,
        scratch_shapes=[
            pltpu.VMEM((rows, depth), bf16),
            pltpu.VMEM((3, rows, depth), bf16),
            pltpu.VMEM((1, depth), f32),
            pltpu.VMEM((2, 1, depth), f32),
            pltpu.VMEM((6, depth, width), bf16),
            pltpu.VMEM((rows + 16, depth), bf16),
            pltpu.VMEM((length, 6 * width), bf16),
            pltpu.VMEM((16, 3 * width), f32),
            pltpu.VMEM((length // BLOCK, 2 * BLOCK, width), f32),
            pltpu.VMEM((8, 48, PAIR), f32),
            pltpu.VMEM((length, width), f32),
            pltpu.VMEM((length, width), f32),
            pltpu.VMEM((length, width), f32),
            pltpu.VMEM((8, 48, PAIR), f32),
            pltpu.VMEM((48, PAIR), f32),
            pltpu.VMEM((8, 48, PAIR), f32),
            pltpu.VMEM((8, 256, PAIR), bf16),
            pltpu.VMEM((8, 32, PAIR), f32),
            pltpu.VMEM((8, 16, PAIR), f32),
            pltpu.VMEM((8, 16, PAIR), f32),
            pltpu.VMEM((length, width), bf16),
            pltpu.VMEM((4, rows, width), bf16),
            pltpu.VMEM((inner, depth), bf16),
            dma(()), dma((6,)), dma(()), dma((6,)), dma((3, 2)), dma((6,)), dma((2,)),
            dma((8,)), dma((8,)), dma((8,)), dma((8,)), dma((8,)), dma((8,)), dma((4,)), dma((4,)),
        ] + [pltpu.VMEM((length, width), f32)] * 8,
        compiler_params=pltpu.CompilerParams(collective_id=0, has_side_effects=True),
        name="layer",
    )(tokens, gain, *weights, mix, decay_base, rate_base, drift, group_gain, start, w_out)


def per_device(tokens, norm_gain, w_recept, w_key, w_value, w_decay, w_rate, w_gate, shift_mix, decay_base, rate_base,
               decay_drift, group_gain, initial_state, w_out):
    return call_layer(
        tokens, norm_gain.reshape(1, -1), (w_recept, w_key, w_value, w_decay, w_rate, w_gate), shift_mix,
        decay_base.reshape(1, -1), rate_base.reshape(1, -1), decay_drift, group_gain.reshape(1, -1), initial_state, w_out)


def solution(mesh):
    finer = Mesh(mesh.devices.reshape(8, 4, 2, mesh.shape["tp"]), AXES)
    in_specs = (
        P(SP_TP, None),
        P(),
        P(None, "tp"),
        P(None, "tp"),
        P(None, "tp"),
        P(None, "tp"),
        P(None, "tp"),
        P(None, "tp"),
        P(None, "tp"),
        P("tp"),
        P("tp"),
        P(SP),
        P("tp"),
        P("tp", None, None),
        P(),
    )
    return jax.shard_map(
        per_device, mesh=finer, in_specs=in_specs, out_specs=P(SP_TP, None), check_vma=False
    )
```

time: 68.4 us -> 56.9 us (0.83)
  the two profiles are of different devices: /device:TPU:192 before, /device:TPU:32 now
where the time goes in v3:
time: 56.9 us; the launch traced here: 56.5 us
  Pallas kernels  54.7 us (96%)
  local copies, waits for them, and re-layouts  1.77 us (3%)
    pallas_call x1, Pallas kernels, call_layer(): pl.pallas_call(layer, out_shape=jax.ShapeDtypeStruct((rows, depth), bf16)...  54.7 us
    unnamed x1, local copies, waits for them, and re-layouts  1.77 us

profile of v3, /device:TPU:32, one launch (start us, length us, event | category | flops | bytes accessed | tf_op | source)
XLA Modules:
  0.0 56.5 jit_solution(10772897174311942222)
XLA Ops:
  0.0 54.7 %layer.1 = bf16[96,2048]{1,0:T(8,128)(2,1)} custom-call(bf16[96,2048]{1,0:T(8,128)(2,1)} %tokens.1, f32[1,2048]{1,0:T(1,128)} %bitcast.4, bf16[2048,256]{1,0:T(8,128)(2,1)} %wr.1, bf16[2048,256]{1,0:T(8,128)(2,1)} %wk.1, bf16[2048,256]{1,0:T(8,128)(2,1)} %wv.1, bf16[2048,256]{1,0:T(8,128)(2,1)} %wd.1, bf16[2048,256]{1,0:T(8,128)(2,1)} %wa.1, ...), custom_call_target="tpu_custom_call" | custom-call | tf_op jit(solution)/shard_map/layer/pallas_call | solution.py:541
  54.7 1.8 %copy.17 = bf16[96,2048]{1,0:T(8,128)(2,1)} copy(bf16[96,2048]{1,0:T(8,128)(2,1)} %layer.1) | data formatting | bytes 786432

commit v4 on v3

--- a/solution.py
+++ b/solution.py
@@ -202,10 +202,10 @@
     for j in range(pairs):
         for side in range(2):
             head = 2 * j + side
-            packed = pack(both[j][:BLOCK], side)
+            packed = pack(both[j][:BLOCK] - unit_eye(), side).astype(bf16)
             for q in range(2):
                 msg[2 * head + q, 0:32, :] = packed
-                msg[2 * head + q, 32:48, :] = pack(both[j][BLOCK + 32 * q:BLOCK + 32 * (q + 1)], side)
+                msg[2 * head + q, 32:48, :] = pack(both[j][BLOCK + 32 * q:BLOCK + 32 * (q + 1)], side).astype(bf16)
 
 
 def read_chunks(chunks, proj, store, before_s, reads_out, fixed_out, gate_out):
@@ -241,20 +241,60 @@
     return jnp.where(is_low, pltpu.roll(top, HEAD, 1), bottom)
 
 
-def unpack(x):
+def fold(x):
+    half = x.shape[0] // 2
+    is_low = lax.broadcasted_iota(jnp.int32, (half, PAIR), 1) < HEAD
+    return jnp.where(is_low, x[:half], x[half:])
+
+
+def unfold(x):
     is_low = lax.broadcasted_iota(jnp.int32, x.shape, 1) < HEAD
-    return jnp.concatenate([jnp.where(is_low, x, 0.0), jnp.where(is_low, pltpu.roll(x, HEAD, 1), 0.0)], axis=0)
-
-
-def state_lhs(x):
-    hi = x.astype(bf16).astype(f32)
-    joined = hi + pltpu.roll(x - hi, HEAD, 1)
-    return jnp.concatenate([joined.astype(bf16), hi.astype(bf16)], axis=1)
-
-
-def state_rhs(x):
+    other = pltpu.roll(x, HEAD, 1)
+    return jnp.concatenate([jnp.where(is_low, x, other), jnp.where(is_low, other, x)], axis=0)
+
+
+def twice(change):
+    change = change.astype(bf16)
+    return jnp.concatenate([change, change], axis=0)
+
+
+def settled(x):
     hi, lo = split(x)
-    return jnp.concatenate([hi, hi, lo, jnp.zeros_like(lo)], axis=0)
+    return hi.astype(f32) + lo.astype(f32)
+
+
+def through_map(x, change2):
+    is_low = lax.broadcasted_iota(jnp.int32, x.shape, 1) < HEAD
+    hi, lo = (part.astype(f32) for part in split(x))
+    return settled(hi + lo + jnp.dot(jnp.where(is_low, hi, lo).astype(bf16), change2, preferred_element_type=f32))
+
+
+def unit_eye():
+    row = lax.broadcasted_iota(jnp.int32, (HEAD, PAIR), 0)
+    col = lax.rem(lax.broadcasted_iota(jnp.int32, (HEAD, PAIR), 1), HEAD)
+    return (row == col).astype(f32)
+
+
+class Map:
+    def __init__(self, change, added):
+        self.change, self.added = change, added
+        self.operand = twice(change)
+
+    def then(self, later):
+        eye = unit_eye()
+        change = through_map(self.change + eye, later.operand) - eye
+        return Map(change, through_map(self.added, later.operand) + later.added)
+
+    def apply(self, state):
+        return through_map(state, self.operand) + self.added
+
+    def message(self):
+        return jnp.concatenate([fold(self.change), fold(self.added)], axis=0).astype(bf16)
+
+
+def map_of(piece):
+    piece = piece.astype(f32)
+    return Map(unfold(piece[0:32]), unfold(piece[32:48]))
 
 
 def layer(tokens, gain, wr, wk, wv, wd, wa, wg, mix, decay_base, rate_base, drift, group_gain, start, w_out, out,
@@ -420,22 +460,15 @@
     slab[unit] = msg[unit]
     read_chunks((0, 1), proj, store, before_s, reads_s, fixed_s, gate_s)
 
-    row = lax.broadcasted_iota(jnp.int32, (96, PAIR), 0)
-    col = lax.broadcasted_iota(jnp.int32, (96, PAIR), 1)
-    running = (row == col).astype(f32) * (col < HEAD).astype(f32)
     for k in range(8):
         @pl.when(k != unit)
         def _():
             landed(slab, recv1, k).wait_recv()
 
-    for k in range(8):
-        pre_map[k] = state_rhs(running[:HEAD])
-        pre_add[k] = running[HEAD:]
-        piece = slab[k]
-        add = jnp.concatenate([jnp.zeros((HEAD, PAIR), f32), unpack(piece[32:48])], axis=0)
-        running = nn(state_lhs(running), state_rhs(unpack(piece[0:32]))) + add
-    slab_sum[0:32, :] = pack(running[:HEAD], 0)
-    slab_sum[32:48, :] = pack(running[HEAD:], 0)
+    one = [map_of(slab[k]) for k in range(8)]
+    two = [one[2 * k].then(one[2 * k + 1]) for k in range(4)]
+    four = [two[2 * k].then(two[2 * k + 1]) for k in range(2)]
+    slab_sum[...] = four[0].then(four[1]).message()
 
     def onward(d):
         return remote(slab_sum, across.at[z], send2.at[d], recv2.at[z], along(lax.rem(z + d, nz)))
@@ -445,21 +478,25 @@
         def _():
             onward(d).start()
 
+    six = four[0].then(two[2])
+    before = (one[0], two[0], two[0].then(one[2]), four[0], four[0].then(one[4]), six, six.then(one[6]))
+    for k in range(7):
+        pre_map[k] = before[k].operand
+        pre_add[k] = before[k].added
     read_chunks((2, 3, 4, 5), proj, store, before_s, reads_s, fixed_s, gate_s)
     begin = start[me["x"], pl.ds(pl.multiple_of(me["c"] * 32, 32), 32), :]
-    state = jnp.concatenate([begin, jnp.zeros((32, PAIR - HEAD), f32)], axis=1)
+    state = jnp.concatenate([begin, begin], axis=1)
     for k in range(7):
         @pl.when(k < z)
         def _():
             landed(across, recv2, k).wait_recv()
 
+    one = [map_of(jnp.where(k < z, across[k].astype(f32), 0.0)) for k in range(7)]
+    late = one[3].then(one[4]).then(one[5].then(one[6]))
+    state = late.apply(one[1].then(one[2]).apply(one[0].apply(state)))
+    back[0] = fold(state).astype(bf16)
     for k in range(7):
-        piece = across[k]
-        new = nn(state_lhs(state), state_rhs(unpack(piece[0:32]))) + unpack(piece[32:48])
-        state = jnp.where(k < z, new, state)
-    state3 = state_lhs(state)
-    for k in range(8):
-        back[k] = pack(nn(state3, pre_map[k]) + pre_add[k], 0)
+        back[k + 1] = fold(through_map(state, pre_map[k]) + pre_add[k]).astype(bf16)
     third = []
     for d in range(1, 8):
         peer = lax.rem(unit + d, units)
@@ -477,31 +514,36 @@
     for j in range(width // PAIR):
         parts = []
         for q in range(2):
-            a, b = entering[4 * j + q], entering[4 * j + 2 + q]
+            a, b = entering[4 * j + q].astype(f32), entering[4 * j + 2 + q].astype(f32)
             parts.append(jnp.where(is_low, a, pltpu.roll(b, HEAD, 1)))
             parts.append(jnp.where(is_low, pltpu.roll(a, HEAD, 1), b))
-        turned.append(rhs_nt(jnp.concatenate(parts, axis=0), masks))
+        diagonal = diag_parts(jnp.concatenate(parts, axis=0), masks)[0]
+        turned.append(jnp.concatenate([diagonal, diagonal], axis=1))
 
     def share(k):
         return pl.ds(pl.multiple_of(k * rows, 16), rows)
 
-    def gate_rows(at_rows):
-        for j in range(width // PAIR):
-            cols = slice(j * PAIR, (j + 1) * PAIR)
-            mixed = fixed_s[at_rows, cols] + nt(lhs3(reads_s[at_rows, cols]), turned[j])
-            center = mixed - head_sum(mixed, masks) * (1.0 / HEAD)
-            spread = head_sum(center * center, masks) * (1.0 / HEAD)
-            scaled = center * lax.rsqrt(spread + GROUP_FLOOR) * group_gain[:, cols]
-            gated[at_rows, cols] = (scaled * gate_s[at_rows, cols]).astype(bf16)
+    def gate_rows(areas):
+        units = [(at_rows, j) for at_rows in areas for j in range(width // PAIR)]
+
+        def cols(j):
+            return slice(j * PAIR, (j + 1) * PAIR)
+
+        mixed = [fixed_s[r, cols(j)] + nt(jnp.concatenate(split(reads_s[r, cols(j)]), axis=1), turned[j]) for r, j in units]
+        center = [m - head_sum(m, masks) * (1.0 / HEAD) for m in mixed]
+        spread = [head_sum(m * m, masks) * (1.0 / HEAD) for m in center]
+        for (r, j), m, v in zip(units, center, spread):
+            scaled = m * lax.rsqrt(v + GROUP_FLOOR) * group_gain[:, cols(j)]
+            gated[r, cols(j)] = (scaled * gate_s[r, cols(j)]).astype(bf16)
 
     fourth = {}
     for d in (2, 1, 3):
         peer = lax.rem(y + d, ny)
-        gate_rows(share(peer))
         fourth[d] = remote(gated.at[share(peer)], token_rows.at[d], send4.at[d], recv4.at[d], {"tp": peer})
+    gate_rows([share(lax.rem(y + d, ny)) for d in (2, 1, 3)])
     for d in (2, 1, 3):
         fourth[d].start()
-    gate_rows(share(y))
+    gate_rows([share(y)])
     out_copy.wait()
 
     def product(block, owner):
@@ -553,17 +595,17 @@
             pltpu.VMEM((length, 6 * width), bf16),
             pltpu.VMEM((16, 3 * width), f32),
             pltpu.VMEM((length // BLOCK, 2 * BLOCK, width), f32),
-            pltpu.VMEM((8, 48, PAIR), f32),
+            pltpu.VMEM((8, 48, PAIR), bf16),
             pltpu.VMEM((length, width), f32),
             pltpu.VMEM((length, width), f32),
             pltpu.VMEM((length, width), f32),
-            pltpu.VMEM((8, 48, PAIR), f32),
-            pltpu.VMEM((48, PAIR), f32),
-            pltpu.VMEM((8, 48, PAIR), f32),
-            pltpu.VMEM((8, 256, PAIR), bf16),
-            pltpu.VMEM((8, 32, PAIR), f32),
-            pltpu.VMEM((8, 16, PAIR), f32),
-            pltpu.VMEM((8, 16, PAIR), f32),
+            pltpu.VMEM((8, 48, PAIR), bf16),
+            pltpu.VMEM((48, PAIR), bf16),
+            pltpu.VMEM((8, 48, PAIR), bf16),
+            pltpu.VMEM((7, PAIR, PAIR), bf16),
+            pltpu.VMEM((7, 32, PAIR), f32),
+            pltpu.VMEM((8, 16, PAIR), bf16),
+            pltpu.VMEM((8, 16, PAIR), bf16),
             pltpu.VMEM((length, width), bf16),
             pltpu.VMEM((4, rows, width), bf16),
             pltpu.VMEM((inner, depth), bf16),

time: 56.9 us -> 52 us (0.914)
  Pallas kernels: 54.7 us -> 49.9 us
    pallas_call x1, Pallas kernels: 54.7 us -> 49.9 us  [call_layer(): pl.pallas_call(layer, out_shape=jax.ShapeDtypeStruct((rows, depth), bf16)...]
where the time goes in v4:
time: 52 us; the launch traced here: 51.7 us
  Pallas kernels  49.9 us (96%)
  local copies, waits for them, and re-layouts  1.77 us (3%)
    pallas_call x1, Pallas kernels, call_layer(): pl.pallas_call(layer, out_shape=jax.ShapeDtypeStruct((rows, depth), bf16)...  49.9 us
    unnamed x1, local copies, waits for them, and re-layouts  1.77 us

profile of v4, /device:TPU:32, one launch (start us, length us, event | category | flops | bytes accessed | tf_op | source)
XLA Modules:
  0.0 51.7 jit_solution(11573306235888585340)
XLA Ops:
  0.0 49.9 %layer.1 = bf16[96,2048]{1,0:T(8,128)(2,1)} custom-call(bf16[96,2048]{1,0:T(8,128)(2,1)} %tokens.1, f32[1,2048]{1,0:T(1,128)} %bitcast.4, bf16[2048,256]{1,0:T(8,128)(2,1)} %wr.1, bf16[2048,256]{1,0:T(8,128)(2,1)} %wk.1, bf16[2048,256]{1,0:T(8,128)(2,1)} %wv.1, bf16[2048,256]{1,0:T(8,128)(2,1)} %wd.1, bf16[2048,256]{1,0:T(8,128)(2,1)} %wa.1, ...), custom_call_target="tpu_custom_call" | custom-call | tf_op jit(solution)/shard_map/layer/pallas_call | solution.py:583
  49.9 1.8 %copy.17 = bf16[96,2048]{1,0:T(8,128)(2,1)} copy(bf16[96,2048]{1,0:T(8,128)(2,1)} %layer.1) | data formatting | bytes 786432

commit v5 on v4

--- a/solution.py
+++ b/solution.py
@@ -75,6 +75,17 @@
 
 def nt(a3, b3):
     return lax.dot_general(a3, b3, (((1,), (1,)), ((), ())), preferred_element_type=f32)
+
+
+def once(a, b, masks):
+    low, high = masks
+    b = b.astype(bf16)
+    return nn(a.astype(bf16), jnp.concatenate([b * low, b * high], axis=0))
+
+
+def settled(x):
+    hi, lo = split(x)
+    return hi.astype(f32) + lo.astype(f32)
 
 
 def tn(a, b):
@@ -161,14 +172,18 @@
         upper_k[block(i), cols(j)] = jnp.where(inclusive, by[u][BLOCK:, PAIR:], 0.0)
         recept_s[block(i), cols(j)] = scaled[u]
         value_s[block(i), cols(j)] = value[u]
-    solved = {u: eye + jnp.where(lax.div(place, 2) == lax.div(other, 2), lower[u], 0.0) for u in units}
-    size = 2
-    while size < BLOCK:
-        inside = jnp.logical_and(
-            lax.div(place, 2 * size) == lax.div(other, 2 * size), lax.div(place, size) != lax.div(other, size))
-        turned = {u: nn(lhs3(solved[u]), rhs_nn(jnp.where(inside, lower[u], 0.0), masks)) for u in units}
-        solved = {u: solved[u] + nn(lhs3(turned[u]), rhs_nn(solved[u], masks)) for u in units}
-        size *= 2
+    inner = {u: jnp.where(lax.div(place, 4) == lax.div(other, 4), lower[u], 0.0) for u in units}
+    square = {u: nn(lhs3(inner[u]), rhs_nn(inner[u], masks)) for u in units}
+    solved = {u: eye + inner[u] + square[u] + nn(lhs3(inner[u]), rhs_nn(square[u], masks)) for u in units}
+    for size in (4, 16):
+        outside = jnp.logical_and(
+            lax.div(place, 4 * size) == lax.div(other, 4 * size), lax.div(place, size) != lax.div(other, size))
+        solved = {u: settled(solved[u]) for u in units}
+        ahead = {u: settled(nn(lhs3(solved[u]), rhs_nn(jnp.where(outside, lower[u], 0.0), masks))) for u in units}
+        grown = {u: nn(lhs3(ahead[u]), jnp.concatenate(
+            [rhs_nn(ahead[u], masks), rhs_nn(solved[u], masks)], axis=1)) for u in units}
+        solved = {u: settled(solved[u] + grown[u][:, PAIR:]) for u in units}
+        solved = {u: solved[u] + nn(lhs3(grown[u][:, :PAIR]), rhs_nn(solved[u], masks)) for u in units}
     both = {u: nn(lhs3(solved[u]), jnp.concatenate([rhs_nn(alpha[u], masks), rhs_nn(pulled[u], masks)], axis=1))
             for u in units}
     for u in units:
@@ -258,11 +273,6 @@
     return jnp.concatenate([change, change], axis=0)
 
 
-def settled(x):
-    hi, lo = split(x)
-    return hi.astype(f32) + lo.astype(f32)
-
-
 def through_map(x, change2):
     is_low = lax.broadcasted_iota(jnp.int32, x.shape, 1) < HEAD
     hi, lo = (part.astype(f32) for part in split(x))
@@ -298,14 +308,13 @@
 
 
 def layer(tokens, gain, wr, wk, wv, wd, wa, wg, mix, decay_base, rate_base, drift, group_gain, start, w_out, out,
-          own, held, last, last_in, wbuf, norm_buf, proj, edge_s, before_s, msg, reads_s, fixed_s, gate_s,
+          own, normed, mate_rows, others, last, last_in, wbuf, proj, edge_s, before_s, msg, reads_s, fixed_s, gate_s,
           slab, slab_sum, across, pre_map, pre_add, back, entering, gated, token_rows, w_out_buf,
           own_sem, w_sem, out_sem, hop_send, hop_recv, edge_send, edge_recv,
-          send1, recv1, send2, recv2, send3, recv3, send4, recv4, *store):
+          send1, recv1, send2, recv2, send3, recv3, send4, recv4, ready_a, ready_b, *store):
     me = here()
     y, z = me["tp"], me["z"]
     ny, nx, nc, nz = lax.axis_size("tp"), lax.axis_size("x"), lax.axis_size("c"), lax.axis_size("z")
-    right, left = lax.rem(y + 1, ny), lax.rem(y + ny - 1, ny)
     far = lax.rem(y + 2, ny)
     unit = me["x"] * nc + me["c"]
     units = nx * nc
@@ -334,81 +343,102 @@
     fetch = pltpu.make_async_copy(tokens, own, own_sem)
     fetch.start()
     w_copies = [pltpu.make_async_copy(w, wbuf.at[i], w_sem.at[i]) for i, w in enumerate((wr, wk, wv, wd, wa, wg))]
+    barrier = pltpu.get_barrier_semaphore()
+    odd = lax.rem(y, 2)
+    mate = y + 1 - 2 * odd
+    beside = lax.rem(y + 2 * odd + ny - 1, ny)
+    x_up, x_down = lax.rem(me["x"] + 1, nx), lax.rem(me["x"] + nx - 1, nx)
+    z_up, z_down = lax.rem(z + 1, nz), lax.rem(z + nz - 1, nz)
+    near = [{"tp": mate}, {"tp": beside}, {"c": 1 - me["c"]}, {"z": z_up}, {"z": z_down}, {"x": x_up}, {"x": x_down}]
+    for to in near:
+        greet(to)
+    for x in (x_up, x_down):
+        greet({"x": x, "c": 1 - me["c"]})
+    ends_stretch = jnp.logical_and(y == ny - 1, seq < total - 1)
+    has_before = seq > 0
+
+    def normalize(x):
+        return (x * lax.rsqrt(jnp.mean(x * x, axis=-1, keepdims=True) + NORM_FLOOR) * gain[...]).astype(bf16)
+
+    fetch.wait()
     for copy in w_copies:
         copy.start()
-    barrier = pltpu.get_barrier_semaphore()
-    for d in range(1, 4):
-        greet({"tp": lax.rem(y + d, ny)})
-    for d in range(1, 8):
-        greet(in_slab(lax.rem(unit + d, units)))
-        greet(along(lax.rem(z + d, nz)))
-    ends_stretch = jnp.logical_and(y == ny - 1, seq < total - 1)
-    has_before = seq > 0
-
-    @pl.when(has_before)
-    def _():
-        greet(at(seq - 1, ny - 1))
-
-    pl.semaphore_wait(barrier, 17 + 4 * ends_stretch.astype(jnp.int32))
-    fetch.wait()
-
-    def part(h):
-        return pl.ds(h * half, half)
-
-    def hop(src, slot, h, to, sem):
-        return remote(src, held.at[slot, part(h)], hop_send.at[sem], hop_recv.at[slot, h], {"tp": to})
-
-    to_right = [hop(own.at[part(h)], 0, h, right, h) for h in (0, 1)]
-    to_left = [hop(own.at[part(h)], 2, h, left, 2 + h) for h in (0, 1)]
-    on_right = hop(held.at[0, part(0)], 1, 0, right, 4)
-    on_left = hop(held.at[2, part(1)], 1, 1, left, 5)
-    to_right[0].start()
-    to_left[1].start()
-    to_right[1].start()
-    to_left[0].start()
-
-    last[...] = own[rows - 16:rows, :].astype(f32)[15:16, :]
-    edges = [remote(last, last_in.at[0], edge_send.at[k], edge_recv.at[0], at(lax.rem(seq + 1, total), k))
-             for k in range(4)]
+    normed[...] = normalize(own[...].astype(f32))
+    last[...] = normed[rows - 16:rows, :].astype(f32)[15:16, :]
+    pl.semaphore_wait(barrier, 9)
+    top, low_half = pl.ds(0, half), pl.ds(half, half)
+
+    def quarter(k):
+        return others.at[pl.ds(k * half, half)]
+
+    def hop(src, dst, sem, to):
+        return remote(src, dst, hop_send.at[sem], hop_recv.at[sem], {"tp": to})
+
+    mate_top = hop(normed.at[top], mate_rows.at[top], 0, mate)
+    mate_low = hop(normed.at[low_half], mate_rows.at[low_half], 1, mate)
+    beside_low = hop(normed.at[low_half], quarter(0), 2, beside)
+    far_top = hop(mate_rows.at[top], quarter(1), 3, beside)
+    beside_top = hop(normed.at[top], quarter(2), 4, beside)
+    far_low = hop(quarter(0), quarter(3), 5, mate)
+    mate_top.start()
+    beside_low.start()
+
+    for to in near:
+        pl.semaphore_signal(ready_a, inc=1, device_id=to, device_id_type=MESH)
+
+    out_copy = pltpu.make_async_copy(w_out, w_out_buf, out_sem)
+    out_copy.start()
+
+    def project(block, parts):
+        for i in range(6):
+            res = jnp.dot(block[...], wbuf[i], preferred_element_type=f32)
+            at_row = 0
+            for base, count in parts:
+                area = pl.ds(pl.multiple_of(base, 16), count)
+                proj[area, width * i:width * (i + 1)] = res[at_row:at_row + count].astype(bf16)
+                at_row += count
+            if block is mate_rows and i < 3:
+                edge_s[:, width * i:width * (i + 1)] = res[rows:].astype(bf16).astype(f32)
+
+    for copy in w_copies:
+        copy.wait()
+    project(normed, [(y * rows, rows)])
+    pl.semaphore_wait(ready_a, 7)
+    for to in near[:3] + near[5:] + [{"z": lax.rem(z + 2, nz)}, {"z": lax.rem(z + nz - 2, nz)}]:
+        pl.semaphore_signal(ready_b, inc=1, device_id=to, device_id_type=MESH)
+
+    edge = remote(last, last_in.at[0], edge_send.at[3], edge_recv.at[0], at(lax.rem(seq + 1, total), ny - 1))
+    spread_edge = [remote(last_in.at[0], last_in.at[0], edge_send.at[k], edge_recv.at[0], {"tp": k}) for k in range(3)]
     inner = [remote(last, last_in.at[1], edge_send.at[4 + k], edge_recv.at[1], {"tp": 2 + k}) for k in range(2)]
+    spreads = jnp.logical_and(y == ny - 1, has_before)
 
     @pl.when(ends_stretch)
     def _():
-        for copy in edges:
-            copy.start()
+        edge.start()
 
     @pl.when(y == 1)
     def _():
         for copy in inner:
             copy.start()
 
-    out_copy = pltpu.make_async_copy(w_out, w_out_buf, out_sem)
-    out_copy.start()
-
-    def normalize(x):
-        return (x * lax.rsqrt(jnp.mean(x * x, axis=-1, keepdims=True) + NORM_FLOOR) * gain[...]).astype(bf16)
-
-    def project(block, owner, with_edge):
-        base = pl.multiple_of(owner * rows, 16)
-        norm_buf[0:rows, :] = normalize(block[...].astype(f32))
-        count = rows + 16 if with_edge else rows
-        for i in range(6):
-            res = jnp.dot(norm_buf[0:count, :], wbuf[i], preferred_element_type=f32)
-            proj[pl.ds(base, rows), width * i:width * (i + 1)] = res[0:rows].astype(bf16)
-            if with_edge and i < 3:
-                edge_s[:, width * i:width * (i + 1)] = res[rows:].astype(bf16).astype(f32)
-
-    for copy in w_copies:
-        copy.wait()
-    project(own, y, False)
-    to_right[0].wait_recv()
-    on_right.start()
-    to_left[1].wait_recv()
-    on_left.start()
-
-    @pl.when(has_before)
-    def _():
-        edges[0].wait_recv()
+    mate_top.wait_send()
+    mate_low.start()
+
+    @pl.when(spreads)
+    def _():
+        edge.wait_recv()
+        for copy in spread_edge:
+            copy.start()
+
+    mate_top.wait_recv()
+    far_top.start()
+    beside_low.wait_recv()
+    mate_low.wait_send()
+    far_low.start()
+
+    @pl.when(jnp.logical_and(y < ny - 1, has_before))
+    def _():
+        edge.wait_recv()
 
     @pl.when(jnp.logical_not(has_before))
     def _():
@@ -422,12 +452,13 @@
     def _():
         last_in[1] = jnp.zeros_like(last)
 
-    norm_buf[rows:, :] = jnp.concatenate(
-        [jnp.broadcast_to(normalize(last_in[k]), (8, own.shape[1])) for k in range(2)], axis=0)
-    to_right[1].wait_recv()
-    project(held.at[0], left, True)
-    to_left[0].wait_recv()
-    project(held.at[2], right, False)
+    mate_rows[rows:, :] = jnp.concatenate(
+        [jnp.broadcast_to(last_in[k], (8, own.shape[1])) for k in range(2)], axis=0).astype(bf16)
+    mate_low.wait_recv()
+    beside_low.wait_send()
+    far_top.wait_send()
+    beside_top.start()
+    project(mate_rows, [(mate * rows, rows)])
 
     group = GROUP * BLOCK
     early = y < 2
@@ -443,9 +474,12 @@
 
     own_base = jnp.where(early, 0, group)
     state_group(own_base, first_edge, proj, mix, decay_base, rate_base, drift, store)
-    on_right.wait_recv()
-    on_left.wait_recv()
-    project(held.at[1], far, False)
+    pl.semaphore_wait(ready_b, 7)
+    far_top.wait_recv()
+    project(others.at[pl.ds(0, rows)], [(beside * rows + half, half), (far * rows, half)])
+    beside_top.wait_recv()
+    far_low.wait_recv()
+    project(others.at[pl.ds(rows, rows)], [(beside * rows, half), (far * rows + half, half)])
     state_group(group - own_base, second_edge, proj, mix, decay_base, rate_base, drift, store)
     compose(store[6], store[7], before_s, msg)
 
@@ -556,7 +590,7 @@
         result = result + product(token_rows[d], lax.rem(y + ny - d, ny))
     out[...] = result.astype(bf16)
 
-    for copy in (*to_right, *to_left, on_right, on_left, *first, *third, *fourth.values()):
+    for copy in (beside_top, far_low, *first, *third, *fourth.values()):
         copy.wait_send()
     for d in range(1, 8):
         @pl.when(z + d < nz)
@@ -565,7 +599,11 @@
 
     @pl.when(ends_stretch)
     def _():
-        for copy in edges:
+        edge.wait_send()
+
+    @pl.when(spreads)
+    def _():
+        for copy in spread_edge:
             copy.wait_send()
 
     @pl.when(y == 1)
@@ -587,11 +625,12 @@
         out_specs=VMEM_SPEC,
         scratch_shapes=[
             pltpu.VMEM((rows, depth), bf16),
-            pltpu.VMEM((3, rows, depth), bf16),
+            pltpu.VMEM((rows, depth), bf16),
+            pltpu.VMEM((rows + 16, depth), bf16),
+            pltpu.VMEM((2 * rows, depth), bf16),
             pltpu.VMEM((1, depth), f32),
             pltpu.VMEM((2, 1, depth), f32),
             pltpu.VMEM((6, depth, width), bf16),
-            pltpu.VMEM((rows + 16, depth), bf16),
             pltpu.VMEM((length, 6 * width), bf16),
             pltpu.VMEM((16, 3 * width), f32),
             pltpu.VMEM((length // BLOCK, 2 * BLOCK, width), f32),
@@ -609,8 +648,9 @@
             pltpu.VMEM((length, width), bf16),
             pltpu.VMEM((4, rows, width), bf16),
             pltpu.VMEM((inner, depth), bf16),
-            dma(()), dma((6,)), dma(()), dma((6,)), dma((3, 2)), dma((6,)), dma((2,)),
+            dma(()), dma((6,)), dma(()), dma((6,)), dma((6,)), dma((6,)), dma((2,)),
             dma((8,)), dma((8,)), dma((8,)), dma((8,)), dma((8,)), dma((8,)), dma((4,)), dma((4,)),
+            pltpu.SemaphoreType.REGULAR, pltpu.SemaphoreType.REGULAR,
         ] + [pltpu.VMEM((length, width), f32)] * 8,
         compiler_params=pltpu.CompilerParams(collective_id=0, has_side_effects=True),
         name="layer",

time: 52 us -> 50.1 us (0.963)
  Pallas kernels: 49.9 us -> 48.1 us
    pallas_call x1, Pallas kernels: 49.9 us -> 48.1 us  [call_layer(): pl.pallas_call(layer, out_shape=jax.ShapeDtypeStruct((rows, depth), bf16)...]
where the time goes in v5:
time: 50.1 us; the launch traced here: 49.9 us
  Pallas kernels  48.1 us (96%)
  local copies, waits for them, and re-layouts  1.77 us (4%)
    pallas_call x1, Pallas kernels, call_layer(): pl.pallas_call(layer, out_shape=jax.ShapeDtypeStruct((rows, depth), bf16)...  48.1 us
    unnamed x1, local copies, waits for them, and re-layouts  1.77 us

profile of v5, /device:TPU:32, one launch (start us, length us, event | category | flops | bytes accessed | tf_op | source)
XLA Modules:
  0.0 49.9 jit_solution(10088650178606851405)
XLA Ops:
  0.0 48.1 %layer.1 = bf16[96,2048]{1,0:T(8,128)(2,1)} custom-call(bf16[96,2048]{1,0:T(8,128)(2,1)} %tokens.1, f32[1,2048]{1,0:T(1,128)} %bitcast.4, bf16[2048,256]{1,0:T(8,128)(2,1)} %wr.1, bf16[2048,256]{1,0:T(8,128)(2,1)} %wk.1, bf16[2048,256]{1,0:T(8,128)(2,1)} %wv.1, bf16[2048,256]{1,0:T(8,128)(2,1)} %wd.1, bf16[2048,256]{1,0:T(8,128)(2,1)} %wa.1, ...), custom_call_target="tpu_custom_call" | custom-call | tf_op jit(solution)/shard_map/layer/pallas_call | solution.py:621
  48.2 1.8 %copy.17 = bf16[96,2048]{1,0:T(8,128)(2,1)} copy(bf16[96,2048]{1,0:T(8,128)(2,1)} %layer.1) | data formatting | bytes 786432

commit v6 on v5

--- a/solution.py
+++ b/solution.py
@@ -69,6 +69,12 @@
     return jnp.concatenate([hi, hi, lo], axis=1)
 
 
+def rhs_turned(x, masks):
+    hi, lo = diag_parts(x, masks)
+    hi, lo = hi.T, lo.T
+    return jnp.concatenate([hi, hi, lo], axis=0)
+
+
 def nn(a3, b3):
     return jnp.dot(a3, b3, preferred_element_type=f32)
 
@@ -159,8 +165,8 @@
         alpha[u] = -unit[u] * jnp.exp(run[u] - logs[u])
         scaled[u] = recept[u] * jnp.exp(run[u])
         left = lhs3(jnp.concatenate([alpha[u], scaled[u]], axis=0))
-        right = jnp.concatenate([rhs_nt(unit_rate * inverse, masks), rhs_nt(key[u] * inverse, masks)], axis=0)
-        by[u] = nt(left, right)
+        right = jnp.concatenate([rhs_turned(unit_rate * inverse, masks), rhs_turned(key[u] * inverse, masks)], axis=1)
+        by[u] = nn(left, right)
         beta_end[u] = unit_rate * to_end
         key_end[u] = key[u] * to_end
     lower = {u: jnp.where(strict, by[u][:BLOCK, :PAIR], 0.0) for u in units}
@@ -197,33 +203,41 @@
         added_s[block(i), cols(j)] = jnp.where(is_low, cross[:BLOCK], cross[BLOCK:])
 
 
-def compose(trans_s, added_s, before_s, msg):
+def compose_half(base, trans_s, added_s, before_s):
     width = trans_s.shape[1]
     pairs = width // PAIR
-    chunks = trans_s.shape[0] // BLOCK
     masks = lane_masks(bf16)
     zero = jnp.zeros((BLOCK, PAIR), f32)
     both = {}
-    for c in range(chunks):
-        block = slice(c * BLOCK, (c + 1) * BLOCK)
+    for c in range(GROUP):
+        block = pl.ds(pl.multiple_of(base + c * BLOCK, BLOCK), BLOCK)
         for j in range(pairs):
             cols = slice(j * PAIR, (j + 1) * PAIR)
             if c == 0:
                 both[j] = jnp.concatenate([trans_s[block, cols], added_s[block, cols]], axis=0)
                 continue
-            before_s[c, :, cols] = both[j]
+            before_s[base // BLOCK + c, :, cols] = both[j]
             both[j] = nn(lhs3(both[j]), rhs_nn(trans_s[block, cols], masks)) + jnp.concatenate(
                 [zero, added_s[block, cols]], axis=0)
-    for j in range(pairs):
+    return both
+
+
+def join_halves(first, second, msg, half_s):
+    masks = lane_masks(bf16)
+    for j in range(len(first)):
+        half_s[:, j * PAIR:(j + 1) * PAIR] = first[j]
+        both = nn(lhs3(first[j]), rhs_nn(second[j][:BLOCK], masks))
+        change = both[:BLOCK] - unit_eye()
+        added = both[BLOCK:] + second[j][BLOCK:]
         for side in range(2):
             head = 2 * j + side
-            packed = pack(both[j][:BLOCK] - unit_eye(), side).astype(bf16)
+            packed = pack(change, side).astype(bf16)
             for q in range(2):
                 msg[2 * head + q, 0:32, :] = packed
-                msg[2 * head + q, 32:48, :] = pack(both[j][BLOCK + 32 * q:BLOCK + 32 * (q + 1)], side).astype(bf16)
-
-
-def read_chunks(chunks, proj, store, before_s, reads_out, fixed_out, gate_out):
+                msg[2 * head + q, 32:48, :] = pack(added[32 * q:32 * (q + 1)], side).astype(bf16)
+
+
+def read_chunks(chunks, proj, store, before_s, half_s, reads_out, fixed_out, gate_out):
     recept_s, value_s, alpha_s, pulled_s, upper_b, upper_k, trans_s, added_s = store
     width = recept_s.shape[1]
     pairs = width // PAIR
@@ -237,9 +251,9 @@
                 [rhs_nn(alpha_s[block, cols], masks), rhs_nn(pulled_s[block, cols], masks)], axis=1))
             reads = recept_s[block, cols] + both[:, :PAIR]
             fixed = both[:, PAIR:] + nn(lhs3(upper_k[block, cols]), rhs_nn(value_s[block, cols], masks))
-            if c > 0:
+            for earlier in ([before_s.at[c]] if c % GROUP else []) + ([half_s] if c >= GROUP else []):
                 both = nt(lhs3(reads), jnp.concatenate(
-                    [rhs_nt(before_s[c, :BLOCK, cols], masks), rhs_nt(before_s[c, BLOCK:, cols], masks)], axis=0))
+                    [rhs_nt(earlier[:BLOCK, cols], masks), rhs_nt(earlier[BLOCK:, cols], masks)], axis=0))
                 reads = both[:, :PAIR]
                 fixed = fixed + both[:, PAIR:]
             reads_out[block, cols] = reads
@@ -308,7 +322,7 @@
 
 
 def layer(tokens, gain, wr, wk, wv, wd, wa, wg, mix, decay_base, rate_base, drift, group_gain, start, w_out, out,
-          own, normed, mate_rows, others, last, last_in, wbuf, proj, edge_s, before_s, msg, reads_s, fixed_s, gate_s,
+          own, normed, mate_rows, others, last, last_in, wbuf, proj, edge_s, before_s, half_s, half_own, msg, reads_s, fixed_s, gate_s,
           slab, slab_sum, across, pre_map, pre_add, back, entering, gated, token_rows, w_out_buf,
           own_sem, w_sem, out_sem, hop_send, hop_recv, edge_send, edge_recv,
           send1, recv1, send2, recv2, send3, recv3, send4, recv4, ready_a, ready_b, *store):
@@ -423,6 +437,8 @@
 
     mate_top.wait_send()
     mate_low.start()
+    beside_low.wait_send()
+    beside_top.start()
 
     @pl.when(spreads)
     def _():
@@ -431,8 +447,9 @@
             copy.start()
 
     mate_top.wait_recv()
+    beside_low.wait_recv()
+    beside_top.wait_send()
     far_top.start()
-    beside_low.wait_recv()
     mate_low.wait_send()
     far_low.start()
 
@@ -455,9 +472,6 @@
     mate_rows[rows:, :] = jnp.concatenate(
         [jnp.broadcast_to(last_in[k], (8, own.shape[1])) for k in range(2)], axis=0).astype(bf16)
     mate_low.wait_recv()
-    beside_low.wait_send()
-    far_top.wait_send()
-    beside_top.start()
     project(mate_rows, [(mate * rows, rows)])
 
     group = GROUP * BLOCK
@@ -474,25 +488,30 @@
 
     own_base = jnp.where(early, 0, group)
     state_group(own_base, first_edge, proj, mix, decay_base, rate_base, drift, store)
+    own_half = compose_half(own_base, store[6], store[7], before_s)
+    for j, both in own_half.items():
+        half_own[:, j * PAIR:(j + 1) * PAIR] = both
     pl.semaphore_wait(ready_b, 7)
     far_top.wait_recv()
-    project(others.at[pl.ds(0, rows)], [(beside * rows + half, half), (far * rows, half)])
     beside_top.wait_recv()
     far_low.wait_recv()
-    project(others.at[pl.ds(rows, rows)], [(beside * rows, half), (far * rows + half, half)])
+    project(others, [(beside * rows + half, half), (far * rows, half), (beside * rows, half), (far * rows + half, half)])
     state_group(group - own_base, second_edge, proj, mix, decay_base, rate_base, drift, store)
-    compose(store[6], store[7], before_s, msg)
+    other_half = compose_half(group - own_base, store[6], store[7], before_s)
+    ours = {j: half_own[:, j * PAIR:(j + 1) * PAIR] for j in other_half}
+    join_halves({j: jnp.where(early, ours[j], other_half[j]) for j in ours},
+                {j: jnp.where(early, other_half[j], ours[j]) for j in ours}, msg, half_s)
 
     def landed(buffer, sems, k):
         return remote(buffer.at[k], buffer.at[k], send1.at[0], sems.at[k], in_slab(unit))
 
     first = []
-    for d in range(1, 8):
+    for d in (4, 3, 5, 2, 6, 1, 7):
         peer = lax.rem(unit + d, units)
         first.append(remote(msg.at[peer], slab.at[unit], send1.at[d], recv1.at[unit], in_slab(peer)))
         first[-1].start()
     slab[unit] = msg[unit]
-    read_chunks((0, 1), proj, store, before_s, reads_s, fixed_s, gate_s)
+    read_chunks((0, 1, 2, 3), proj, store, before_s, half_s, reads_s, fixed_s, gate_s)
 
     for k in range(8):
         @pl.when(k != unit)
@@ -507,7 +526,7 @@
     def onward(d):
         return remote(slab_sum, across.at[z], send2.at[d], recv2.at[z], along(lax.rem(z + d, nz)))
 
-    for d in (4, 3, 2, 1, 5, 6, 7):
+    for d in (4, 5, 3, 6, 2, 7, 1):
         @pl.when(z + d < nz)
         def _():
             onward(d).start()
@@ -517,7 +536,7 @@
     for k in range(7):
         pre_map[k] = before[k].operand
         pre_add[k] = before[k].added
-    read_chunks((2, 3, 4, 5), proj, store, before_s, reads_s, fixed_s, gate_s)
+    read_chunks((4, 5), proj, store, before_s, half_s, reads_s, fixed_s, gate_s)
     begin = start[me["x"], pl.ds(pl.multiple_of(me["c"] * 32, 32), 32), :]
     state = jnp.concatenate([begin, begin], axis=1)
     for k in range(7):
@@ -532,7 +551,7 @@
     for k in range(7):
         back[k + 1] = fold(through_map(state, pre_map[k]) + pre_add[k]).astype(bf16)
     third = []
-    for d in range(1, 8):
+    for d in (4, 3, 5, 2, 6, 1, 7):
         peer = lax.rem(unit + d, units)
         third.append(remote(back.at[peer], entering.at[unit], send3.at[d], recv3.at[unit], in_slab(peer)))
         third[-1].start()
@@ -590,7 +609,7 @@
         result = result + product(token_rows[d], lax.rem(y + ny - d, ny))
     out[...] = result.astype(bf16)
 
-    for copy in (beside_top, far_low, *first, *third, *fourth.values()):
+    for copy in (far_top, far_low, *first, *third, *fourth.values()):
         copy.wait_send()
     for d in range(1, 8):
         @pl.when(z + d < nz)
@@ -634,6 +653,8 @@
             pltpu.VMEM((length, 6 * width), bf16),
             pltpu.VMEM((16, 3 * width), f32),
             pltpu.VMEM((length // BLOCK, 2 * BLOCK, width), f32),
+            pltpu.VMEM((2 * BLOCK, width), f32),
+            pltpu.VMEM((2 * BLOCK, width), f32),
             pltpu.VMEM((8, 48, PAIR), bf16),
             pltpu.VMEM((length, width), f32),
             pltpu.VMEM((length, width), f32),

time: 50.1 us -> 49 us (0.978)
  Pallas kernels: 48.1 us -> 47 us
    pallas_call x1, Pallas kernels: 48.1 us -> 47 us  [call_layer(): pl.pallas_call(layer, out_shape=jax.ShapeDtypeStruct((rows, depth), bf16)...]
where the time goes in v6:
time: 49 us; the launch traced here: 48.8 us
  Pallas kernels  47 us (96%)
  local copies, waits for them, and re-layouts  1.77 us (4%)
    pallas_call x1, Pallas kernels, call_layer(): pl.pallas_call(layer, out_shape=jax.ShapeDtypeStruct((rows, depth), bf16)...  47 us
    unnamed x1, local copies, waits for them, and re-layouts  1.77 us

profile of v6, /device:TPU:32, one launch (start us, length us, event | category | flops | bytes accessed | tf_op | source)
XLA Modules:
  0.0 48.8 jit_solution(9288881441316498601)
XLA Ops:
  0.0 47.0 %layer.1 = bf16[96,2048]{1,0:T(8,128)(2,1)} custom-call(bf16[96,2048]{1,0:T(8,128)(2,1)} %tokens.1, f32[1,2048]{1,0:T(1,128)} %bitcast.4, bf16[2048,256]{1,0:T(8,128)(2,1)} %wr.1, bf16[2048,256]{1,0:T(8,128)(2,1)} %wk.1, bf16[2048,256]{1,0:T(8,128)(2,1)} %wv.1, bf16[2048,256]{1,0:T(8,128)(2,1)} %wd.1, bf16[2048,256]{1,0:T(8,128)(2,1)} %wa.1, ...), custom_call_target="tpu_custom_call" | custom-call | tf_op jit(solution)/shard_map/layer/pallas_call | solution.py:640
  47.0 1.8 %copy.17 = bf16[96,2048]{1,0:T(8,128)(2,1)} copy(bf16[96,2048]{1,0:T(8,128)(2,1)} %layer.1) | data formatting | bytes 786432

commit v7 on v6

--- a/solution.py
+++ b/solution.py
@@ -94,12 +94,9 @@
     return hi.astype(f32) + lo.astype(f32)
 
 
-def tn(a, b):
-    a_hi, a_lo = split(a)
-    b_hi, b_lo = split(b)
+def turned_once(a, b):
     return lax.dot_general(
-        jnp.concatenate([a_hi, a_lo, a_hi], axis=0), jnp.concatenate([b_hi, b_hi, b_lo], axis=0),
-        (((0,), (0,)), ((), ())), preferred_element_type=f32)
+        a.astype(bf16), b.astype(bf16), (((0,), (0,)), ((), ())), preferred_element_type=f32)
 
 
 def head_sum(x, masks):
@@ -196,10 +193,10 @@
         i, j = u
         alpha_s[block(i), cols(j)] = both[u][:, :PAIR]
         pulled_s[block(i), cols(j)] = both[u][:, PAIR:]
-        cross = tn(both[u][:, :PAIR], beta_end[u])
+        cross = turned_once(both[u][:, :PAIR], beta_end[u])
         trans_s[block(i), cols(j)] = jnp.where(is_low, cross[:BLOCK], cross[BLOCK:]) + eye * jnp.exp(run[u][BLOCK - 1:BLOCK, :])
-        cross = tn(jnp.concatenate([both[u][:, PAIR:], value[u]], axis=0),
-                   jnp.concatenate([beta_end[u], key_end[u]], axis=0))
+        cross = turned_once(jnp.concatenate([both[u][:, PAIR:], value[u]], axis=0),
+                            jnp.concatenate([beta_end[u], key_end[u]], axis=0))
         added_s[block(i), cols(j)] = jnp.where(is_low, cross[:BLOCK], cross[BLOCK:])
 
 

time: 49 us -> 48.7 us (level)
  no operation moved by 1% of the time
where the time goes in v7:
time: 48.7 us; the launch traced here: 48.5 us
  Pallas kernels  46.8 us (96%)
  local copies, waits for them, and re-layouts  1.77 us (4%)
    pallas_call x1, Pallas kernels, call_layer(): pl.pallas_call(layer, out_shape=jax.ShapeDtypeStruct((rows, depth), bf16)...  46.8 us
    unnamed x1, local copies, waits for them, and re-layouts  1.77 us

profile of v7, /device:TPU:32, one launch (start us, length us, event | category | flops | bytes accessed | tf_op | source)
XLA Modules:
  0.0 48.5 jit_solution(3213080456748087160)
XLA Ops:
  0.0 46.8 %layer.1 = bf16[96,2048]{1,0:T(8,128)(2,1)} custom-call(bf16[96,2048]{1,0:T(8,128)(2,1)} %tokens.1, f32[1,2048]{1,0:T(1,128)} %bitcast.4, bf16[2048,256]{1,0:T(8,128)(2,1)} %wr.1, bf16[2048,256]{1,0:T(8,128)(2,1)} %wk.1, bf16[2048,256]{1,0:T(8,128)(2,1)} %wv.1, bf16[2048,256]{1,0:T(8,128)(2,1)} %wd.1, bf16[2048,256]{1,0:T(8,128)(2,1)} %wa.1, ...), custom_call_target="tpu_custom_call" | custom-call | tf_op jit(solution)/shard_map/layer/pallas_call | solution.py:637
  46.8 1.8 %copy.17 = bf16[96,2048]{1,0:T(8,128)(2,1)} copy(bf16[96,2048]{1,0:T(8,128)(2,1)} %layer.1) | data formatting | bytes 786432
